TPU v7x, 1024 devices: a whole 4x8x16 slice. The times are simulated.
1024 devices in a mesh: rep: 16 (over z), fs: 8 (over y), tp: 8 (over x, core).
Axes of the slice: x: 4, y: 8, z: 16, core: 2. Of those that a mesh axis runs over, the one named last changes fastest.
Arguments:
- tokens: bfloat16 [6144, 2048], P('rep', ('fs', 'tp')), may hold values from -6 to 6
- cotangent: bfloat16 [6144, 2048], P('rep', ('fs', 'tp')), may hold values from -16 to 16
- gain: float32 [2048], replicated, may hold values from 0.1 to 1.9
- w_gate: bfloat16 [5376, 2048], P(('fs', 'tp')), may hold values from -0.125 to 0.125
- w_up: bfloat16 [5376, 2048], P(('fs', 'tp')), may hold values from -0.125 to 0.125
- w_down: bfloat16 [5376, 2048], P(('fs', 'tp')), may hold values from -0.078125 to 0.078125
Outputs:
- grad_input: bfloat16 [6144, 2048], P('rep', ('fs', 'tp'))
- grad_gain: float32 [2048], P(('fs', 'tp'))
- grad_gate: float32 [5376, 2048], P(('fs', 'tp'))
- grad_up: float32 [5376, 2048], P(('fs', 'tp'))
- grad_down: float32 [5376, 2048], P(('fs', 'tp'))
All inputs are finite; a program needn't handle non-finite values.
Results may differ from a plain program's by a relative error of at most 0.006.
Values may be sent and summed in bfloat16 or wider, within the bound.
No kernel may reach another device: no remote copies, remote signals or barrier semaphores. Data moves between devices by JAX's collectives and lax.ppermute only.
A program may use at most 64 MiB of HBM per device.

v0:
```python
import functools

import jax
import jax.numpy as jnp
from jax import lax
from jax.experimental import pallas as pl
from jax.experimental.pallas import tpu as pltpu
from jax.sharding import Mesh
from jax.sharding import PartitionSpec as P


FS_TP = ("fs", "tp_0", "tp_1")
EPS = 1e-06
BF = jnp.bfloat16
F32 = jnp.float32
LANES = 128
VMEM = pl.BlockSpec(memory_space=pltpu.VMEM)


def gain_columns(gain_ref, out_ref):
    for q in range(gain_ref.shape[0]):
        row = jnp.broadcast_to(gain_ref[q : q + 1, :], (LANES, LANES))
        out_ref[q * LANES : (q + 1) * LANES, :] = row.T


def split_in_two(v):
    high = v.astype(BF)
    return high, (v - high.astype(F32)).astype(BF)


def main_kernel(
    sizes,
    own_ref,
    other_ref,
    gate_w_ref,
    up_w_ref,
    down_w_ref,
    gain_ref,
    keep_ref,
    send_ref,
    row_ref,
    inv_ref,
    far_ref,
    near_ref,
    back_ref,
    stay_ref,
    normed_s,
    cot_s,
    pair_s,
    down_s,
    delta_s,
    hidden_s,
    gain_s,
    part_s,
    grad_s,
):
    n_rep, n_fs, n_x, n_core, tokens, hidden, padded, width, block = sizes
    core = lax.axis_index("tp_1")
    z = lax.axis_index("rep")
    tall = grad_s.shape[1]

    low = padded - 16
    pair_s[low:padded, :] = jnp.zeros((16, width), BF)
    pair_s[padded + low : 2 * padded, :] = jnp.zeros((16, width), BF)
    down_s[low:padded, :] = jnp.zeros((16, width), BF)
    pair_s[0:hidden, :] = gate_w_ref[...]
    pair_s[padded : padded + hidden, :] = up_w_ref[...]
    down_s[0:hidden, :] = down_w_ref[...]
    gain_columns(gain_ref, gain_s)

    def square_sum(s, acc):
        for ref in (own_ref, other_ref):
            v = ref[s, :, 0:tokens].astype(F32)
            v = v * v
            for k in range(block // 8):
                acc = acc + v[8 * k : 8 * k + 8, :]
        return acc

    total = lax.fori_loop(0, n_fs * n_x, square_sum, jnp.zeros((8, tokens), F32))
    mean = jnp.sum(total, axis=0, keepdims=True) / width
    inv = lax.rsqrt(mean + EPS)
    inv_ref[...] = jnp.broadcast_to(inv, (8, tokens))

    def normalise(s, carry):
        x = s // n_fs
        y = s % n_fs
        for ref, which in ((own_ref, core), (other_ref, 1 - core)):
            at = pl.multiple_of(((y * n_x + x) * n_core + which) * block, block)
            v = ref[s, :, 0:tokens].astype(F32) * inv
            g = gain_s[pl.ds(at, block), :]
            v = v * jnp.concatenate([g] * (tokens // LANES), axis=1)
            normed_s[pl.ds(at, block), :] = v.astype(BF)
            cot_s[pl.ds(at, block), :] = ref[s, :, tokens : 2 * tokens]
        return carry

    lax.fori_loop(0, n_fs * n_x, normalise, 0)

    both = jnp.dot(pair_s[...], normed_s[...], preferred_element_type=F32)
    d_hidden = 0.5 * jnp.dot(down_s[...], cot_s[...], preferred_element_type=F32)
    gate = both[0:padded, :]
    up = both[padded : 2 * padded, :]
    sig = jax.nn.sigmoid(gate)
    active = gate * sig
    hidden_s[...] = (active * up).astype(BF)
    d_gate = (d_hidden * up * sig * (1.0 + gate * (1.0 - sig))).astype(BF)
    d_up = (d_hidden * active).astype(BF)
    delta_s[0:padded, :] = d_gate
    delta_s[padded : 2 * padded, :] = d_up
    row = jnp.sum(d_gate.astype(F32) * gate + d_up.astype(F32) * up, axis=0, keepdims=True)
    row_ref[...] = jnp.broadcast_to(row, (8, tokens))
    high, low_part = split_in_two(row)
    send_ref[n_fs * n_x] = jnp.concatenate(
        [high, low_part, jnp.zeros((block - 2, tokens), BF)], axis=0
    )

    step = 256
    for b in range(width // step):
        cols = slice(b * step, (b + 1) * step)
        value = lax.dot_general(
            pair_s[:, cols], delta_s[...], (((0,), (0,)), ((), ())), preferred_element_type=F32
        ).astype(BF)
        for k in range(step // block):
            part_s[b * (step // block) + k] = value[k * block : (k + 1) * block, :]

    def share(s, carry):
        keep_ref[s] = part_s[n_core * s + core]
        send_ref[s] = part_s[n_core * s + 1 - core]
        return carry

    lax.fori_loop(0, n_fs * n_x, share, 0)

    for b in range(width // step):
        rows = slice(b * step, (b + 1) * step)
        two = lax.dot_general(
            delta_s[...], normed_s[rows, :], (((1,), (1,)), ((), ())), preferred_element_type=F32
        )
        one = 0.5 * lax.dot_general(
            hidden_s[...], cot_s[rows, :], (((1,), (1,)), ((), ())), preferred_element_type=F32
        )
        for k in range(step // LANES):
            at = b * (step // LANES) + k
            lanes = slice(k * LANES, (k + 1) * LANES)
            grad_s[at, :, 0:LANES] = two[0:tall, lanes]
            grad_s[at, :, LANES : 2 * LANES] = two[padded : padded + tall, lanes]
            grad_s[at, :, 2 * LANES : 3 * LANES] = one[0:tall, lanes]

    side = 1 - 2 * core
    for i in range(4):
        for ref, base in ((far_ref, 4), (near_ref, 3), (back_ref, 1), (stay_ref, 2)):
            chunk = lax.rem(z + side * (base + 4 * i) + 2 * n_rep, n_rep)
            ref[i] = grad_s[chunk].astype(ref.dtype)


def core_kernel(block, keep_ref, got_ref, row_ref, out_ref):
    slabs = keep_ref.shape[0]
    tokens = keep_ref.shape[2]
    other = got_ref[slabs, 0:8, :].astype(F32)
    row = row_ref[0:1, :] + other[0:1, :] + other[1:2, :]
    high, low_part = split_in_two(row)
    tail = jnp.concatenate([high, low_part, jnp.zeros((6, tokens), BF)], axis=0)

    def add(s, carry):
        v = keep_ref[s].astype(F32) + got_ref[s].astype(F32)
        out_ref[s, 0:block, :] = v.astype(BF)
        out_ref[s, block : block + 8, :] = tail
        return carry

    lax.fori_loop(0, slabs, add, 0)


def stop_kernel(far_ref, near_ref, back_ref, stay_ref, *out_refs):
    for i, out_ref in enumerate(out_refs):
        v = stay_ref[i] + far_ref[i].astype(F32) + near_ref[i].astype(F32) + back_ref[i].astype(F32)
        out_ref[...] = v.astype(BF)


def owner_kernel(
    sizes,
    part_ref,
    tok_ref,
    cot_ref,
    inv_ref,
    gain_ref,
    a_ref,
    b_ref,
    c_ref,
    d_ref,
    input_ref,
    chunk_ref,
    gain_s,
):
    n_x, n_core, width, hidden, block = sizes
    sources, rows, tokens = part_ref.shape
    me = (lax.axis_index("fs") * n_x + lax.axis_index("tp_0")) * n_core + lax.axis_index("tp_1")
    gain_columns(gain_ref, gain_s)

    def add(s, acc):
        return acc + part_ref[s].astype(F32)

    total = lax.fori_loop(0, sources, add, jnp.zeros((rows, tokens), F32))
    summed = total[0:block, :]
    row = (total[block : block + 1, :] + total[block + 1 : block + 2, :]) / width
    inv = inv_ref[0:1, :]
    g = gain_s[pl.ds(pl.multiple_of(me * block, block), block), :]
    d_unit = summed * jnp.concatenate([g] * (tokens // LANES), axis=1)
    unit = tok_ref[...].astype(F32) * inv
    input_ref[...] = (cot_ref[...].astype(F32) + inv * (d_unit - unit * row)).astype(BF)

    along = jnp.sum(unit * summed, axis=1, keepdims=True)
    square = jnp.concatenate(
        [jnp.broadcast_to(along, (block, LANES)), jnp.zeros((LANES - block, LANES), F32)], axis=0
    )
    v = square.T[0:8, :]
    high, mid = split_in_two(v)
    low = v - high.astype(F32) - mid.astype(F32)
    extra = jnp.concatenate([high.astype(F32), mid.astype(F32), low], axis=1)[0:1, :]
    chunk = a_ref[...].astype(F32) + b_ref[...].astype(F32) + c_ref[...].astype(F32) + d_ref[...].astype(F32)
    which = lax.broadcasted_iota(jnp.int32, chunk.shape, 0)
    chunk = jnp.where(which == hidden, jnp.broadcast_to(extra, chunk.shape), chunk)
    chunk_ref[...] = chunk[0 : hidden + 1, :].astype(BF)


def out_kernel(all_ref, gate_ref, up_ref, down_ref, gain_ref):
    n, tall, _ = all_ref.shape
    hidden = tall - 1
    total = jnp.zeros((1, 3 * LANES), F32)
    for b in range(n):
        lanes = slice(b * LANES, (b + 1) * LANES)
        v = all_ref[b].astype(F32)
        gate_ref[:, lanes] = v[0:hidden, 0:LANES]
        up_ref[:, lanes] = v[0:hidden, LANES : 2 * LANES]
        down_ref[:, lanes] = v[0:hidden, 2 * LANES : 3 * LANES]
        total = total + v[hidden : hidden + 1, :]
    gain = total[:, 0:LANES] + total[:, LANES : 2 * LANES] + total[:, 2 * LANES : 3 * LANES]
    gain_ref[...] = gain[:, 0 : gain_ref.shape[1]]


def spread(block, axis):
    n = lax.axis_size(axis)
    copies = jnp.broadcast_to(block[None], (n,) + block.shape)
    return lax.all_to_all(copies, axis, 0, 0, tiled=True)


def shifted(v, by):
    n = lax.axis_size("rep")
    pairs = []
    for z in range(n):
        pairs.append((z * 2, (z + by) % n * 2))
        pairs.append((z * 2 + 1, (z - by) % n * 2 + 1))
    return lax.ppermute(v, ("rep", "tp_1"), pairs)


def body(tokens, cotangent, gain, w_gate, w_up, w_down):
    n_rep = lax.axis_size("rep")
    n_fs, n_x, n_core = (lax.axis_size(a) for a in FS_TP)
    peers = n_fs * n_x
    rows, block = tokens.shape
    width = gain.shape[0]
    hidden = w_gate.shape[0]
    padded = -(-hidden // 32) * 32
    tall = -(-hidden // 8) * 8
    n_blocks = width // LANES
    tok_t, cot_t = tokens.T, cotangent.T
    both = jnp.concatenate([tok_t, cot_t], axis=1)
    column = spread(both, "fs")
    plane = spread(column.reshape(n_fs * block, 2 * rows), "tp_0")
    plane = plane.reshape(peers, block, 2 * rows)
    other = lax.ppermute(plane, "tp_1", [(0, 1), (1, 0)])
    gain_rows = gain.reshape(n_blocks, LANES)

    def shape(*dims, dtype=BF):
        return jax.ShapeDtypeStruct(dims, dtype)

    sizes = (n_rep, n_fs, n_x, n_core, rows, hidden, padded, width, block)
    group = (4, tall, 3 * LANES)
    keep, send, row, inv, far, near, back, stay = pl.pallas_call(
        functools.partial(main_kernel, sizes),
        out_shape=[
            shape(peers, block, rows),
            shape(peers + 1, block, rows),
            shape(8, rows, dtype=F32),
            shape(8, rows, dtype=F32),
            shape(*group),
            shape(*group),
            shape(*group),
            shape(*group, dtype=F32),
        ],
        in_specs=[VMEM] * 6,
        out_specs=[VMEM] * 8,
        scratch_shapes=[
            pltpu.VMEM((width, rows), BF),
            pltpu.VMEM((width, rows), BF),
            pltpu.VMEM((2 * padded, width), BF),
            pltpu.VMEM((padded, width), BF),
            pltpu.VMEM((2 * padded, rows), BF),
            pltpu.VMEM((padded, rows), BF),
            pltpu.VMEM((width, LANES), F32),
            pltpu.VMEM((peers * n_core, block, rows), BF),
            pltpu.VMEM((n_blocks, tall, 3 * LANES), F32),
        ],
        compiler_params=pltpu.CompilerParams(vmem_limit_bytes=34 * 2**20),
        cost_estimate=pl.CostEstimate(flops=11 * 10**8, bytes_accessed=10**7, transcendentals=0),
        name="main",
    )(plane, other, w_gate, w_up, w_down, gain_rows)

    got = lax.ppermute(send, "tp_1", [(0, 1), (1, 0)])
    far = shifted(far, 2)
    near = shifted(near, 1)
    back = shifted(back, -1)
    ready = pl.pallas_call(
        functools.partial(core_kernel, block),
        out_shape=shape(peers, block + 8, rows),
        in_specs=[VMEM] * 3,
        out_specs=VMEM,
        compiler_params=pltpu.CompilerParams(vmem_limit_bytes=8 * 2**20),
        cost_estimate=pl.CostEstimate(flops=10**6, bytes_accessed=3 * 10**6, transcendentals=0),
        name="core",
    )(keep, got, row)
    parts = lax.all_to_all(ready, FS_TP[:2], 0, 0, tiled=True)
    sums = pl.pallas_call(
        stop_kernel,
        out_shape=[shape(tall, 3 * LANES)] * 4,
        in_specs=[VMEM] * 4,
        out_specs=[VMEM] * 4,
        compiler_params=pltpu.CompilerParams(vmem_limit_bytes=8 * 2**20),
        cost_estimate=pl.CostEstimate(flops=10**6, bytes_accessed=2 * 10**6, transcendentals=0),
        name="stop",
    )(far, near, back, stay)
    sums = [shifted(s, by) for s, by in zip(sums, (2, 6, -6, -2))]

    grad_input, chunk = pl.pallas_call(
        functools.partial(owner_kernel, (n_x, n_core, width, hidden, block)),
        out_shape=[shape(block, rows), shape(hidden + 1, 3 * LANES)],
        in_specs=[VMEM] * 9,
        out_specs=[VMEM] * 2,
        scratch_shapes=[pltpu.VMEM((width, LANES), F32)],
        compiler_params=pltpu.CompilerParams(vmem_limit_bytes=12 * 2**20),
        cost_estimate=pl.CostEstimate(flops=10**8, bytes_accessed=2 * 10**6, transcendentals=0),
        name="owner",
    )(parts, tok_t, cot_t, inv, gain_rows, *sums)
    everything = lax.all_gather(chunk, "rep", axis=0, tiled=False)
    grad_gate, grad_up, grad_down, grad_gain = pl.pallas_call(
        out_kernel,
        out_shape=[shape(hidden, width, dtype=F32)] * 3 + [shape(1, block, dtype=F32)],
        in_specs=[VMEM],
        out_specs=[VMEM] * 4,
        compiler_params=pltpu.CompilerParams(vmem_limit_bytes=12 * 2**20),
        name="out",
    )(everything)
    return (grad_input.T, grad_gain.reshape(block), grad_gate, grad_up, grad_down)


def solution(mesh):
    torus = Mesh(
        mesh.devices.reshape(mesh.shape["rep"], mesh.shape["fs"], 4, 2),
        ("rep", "fs", "tp_0", "tp_1"),
    )
    placed = (P("rep", FS_TP), P("rep", FS_TP), P(), P(FS_TP, None), P(FS_TP, None), P(FS_TP, None))
    return jax.shard_map(
        body,
        mesh=torus,
        in_specs=placed,
        out_specs=(P("rep", FS_TP), P(FS_TP), P(FS_TP, None), P(FS_TP, None), P(FS_TP, None)),
        check_vma=False,
    )
```

profile of v0, /device:TPU:6, one launch (start us, length us, event | category | flops | bytes accessed | tf_op | source)
XLA Modules:
  0.0 157.6 jit_solution(18428274818667221533)
XLA Ops:
  0.6 0.8 pad_maximum_fusion
  1.4 21.6 %all_to_all.15 = bf16[8,32,768]{2,1,0:T(8,128)(2,1)S(1)} all-to-all(bf16[8,32,768]{2,1,0:T(8,128)(2,1)S(1)} %broadcast_in_dim.6), channel_id=1, replica_groups=mesh['rep'=16,'fs'=8,'tp_0'=4,'tp_1'=2] {'fs'}, dimensions={0} | all-to-all | bytes 786432 | tf_op jit(solution)/shard_map/all_to_all | solution.py:241
  23.0 0.1 broadcast_in_dim.15
  23.1 0.0 copy-start
  23.1 0.0 copy-start.1
  23.1 0.0 copy-start.2
  23.2 0.0 copy-start.5
  23.2 22.0 %all_to_all.16 = bf16[4,256,768]{2,1,0:T(8,128)(2,1)S(1)} all-to-all(bf16[4,256,768]{2,1,0:T(8,128)(2,1)S(1)} %broadcast_in_dim.15), channel_id=1, replica_groups=mesh['rep'=16,'fs'=8,'tp_0'=4,'tp_1'=2] {'tp_0'}, dimensions={0} | all-to-all | bytes 3145728 | tf_op jit(solution)/shard_map/all_to_all | solution.py:241
  45.1 1.9 %collective-permute-start = (bf16[32,32,768]{2,1,0:T(8,128)(2,1)S(1)}, bf16[32,32,768]{2,1,0:T(8,128)(2,1)S(1)}, u32[]{:S(2)}, u32[]{:S(2)}) collective-permute-start(bf16[32,32,768]{2,1,0:T(8,128)(2,1)S(1)} %bitcast.8), channel_id=1, source_target_pairs={{0,1},{1,0},{2,3},{3,2},{4,5},{5,4},{6,7},{7,6},{8,9},{9,8},{10,11... | collective-permute-start | bytes 4718600 | tf_op jit(solution)/shard_map/ppermute | solution.py:268
  47.0 3.4 %collective-permute-done.other_ref = bf16[32,32,768]{2,1,0:T(8,128)(2,1)S(1)} collective-permute-done((bf16[32,32,768]{2,1,0:T(8,128)(2,1)S(1)}, bf16[32,32,768]{2,1,0:T(8,128)(2,1)S(1)}, u32[]{:S(2)}, u32[]{:S(2)}) %collective-permute-start) | collective-permute-done | bytes 1572896 | tf_op jit(solution)/shard_map/ppermute | solution.py:268
  50.4 0.0 copy-done
  50.4 0.0 copy-done.1
  50.4 0.0 copy-done.2
  50.4 0.0 copy-done.5
  50.4 4.6 %main.1 = (bf16[32,32,384]{2,1,0:T(8,128)(2,1)S(1)}, bf16[33,32,384]{2,1,0:T(8,128)(2,1)S(1)}, f32[8,384]{1,0:T(8,128)S(1)}, f32[8,384]{1,0:T(8,128)S(1)}, bf16[...) custom-call(bf16[32,32,768]{2,1,0:T(8,128)(2,1)S(1)} %bitcast.9, ...), custom_call_target="tpu_custom_call" | custom-call | flops 1100000000 | bytes 10000000 | tf_op jit(solution)/shard_map/main/pallas_call | solution.py:276
  55.0 2.0 %collective-permute-start.1 = (bf16[33,32,384]{2,1,0:T(8,128)(2,1)S(1)}, bf16[33,32,384]{2,1,0:T(8,128)(2,1)S(1)}, u32[]{:S(2)}, u32[]{:S(2)}) collective-permute-start(bf16[33,32,384]{2,1,0:T(8,128)(2,1)S(1)} %get-tuple-element.24), channel_id=1, source_target_pairs={{0,1},{1,0},{2,3},{3,2},{4,5},{5,4},{6,7},{7,6},{8,9},{9,8},{10,11... | collective-permute-start | bytes 2433032 | tf_op jit(solution)/shard_map/ppermute | solution.py:306
  57.1 2.2 %collective-permute-done.1.got_ref = bf16[33,32,384]{2,1,0:T(8,128)(2,1)S(1)} collective-permute-done((bf16[33,32,384]{2,1,0:T(8,128)(2,1)S(1)}, bf16[33,32,384]{2,1,0:T(8,128)(2,1)S(1)}, u32[]{:S(2)}, u32[]{:S(2)}) %collective-permute-start.1) | collective-permute-done | bytes 811040 | tf_op jit(solution)/shard_map/ppermute | solution.py:306
  59.2 1.3 core.1
  60.5 0.0 copy-start.3
  60.5 0.0 copy-start.4
  60.5 5.8 %all-to-all-start.2 = ((bf16[32,40,384]{2,1,0:T(8,128)(2,1)}), bf16[32,40,384]{2,1,0:T(8,128)(2,1)S(1)}, u32[]{:S(2)}, u32[]{:S(2)}) async-start(bf16[32,40,384]{2,1,0:T(8,128)(2,1)} %core.1), calls=%async_computation.2 | async-start | bytes 1966080 | tf_op jit(solution)/shard_map/all_to_all | solution.py:319
  66.4 6.1 %collective-permute-start.2 = (bf16[4,88,384]{2,1,0:T(8,128)(2,1)S(1)}, bf16[4,88,384]{2,1,0:T(8,128)(2,1)S(1)}, u32[]{:S(2)}, u32[]{:S(2)}) collective-permute-start(bf16[4,88,384]{2,1,0:T(8,128)(2,1)S(1)} %get-tuple-element.27), channel_id=1, source_target_pairs={{0,128},{1,897},{64,192},{65,961},{128,256},{129,1},{192,320},{193... | collective-permute-start | bytes 811016 | tf_op jit(solution)/shard_map/ppermute | solution.py:250
  72.5 4.3 %collective-permute-start.3 = (bf16[4,88,384]{2,1,0:T(8,128)(2,1)S(1)}, bf16[4,88,384]{2,1,0:T(8,128)(2,1)S(1)}, u32[]{:S(2)}, u32[]{:S(2)}) collective-permute-start(bf16[4,88,384]{2,1,0:T(8,128)(2,1)S(1)} %get-tuple-element.28), channel_id=1, source_target_pairs={{0,64},{1,961},{64,128},{65,1},{128,192},{129,65},{192,256},{193,1... | collective-permute-start | bytes 811016 | tf_op jit(solution)/shard_map/ppermute | solution.py:250
  76.8 11.7 %collective-permute-start.4 = (bf16[4,88,384]{2,1,0:T(8,128)(2,1)S(1)}, bf16[4,88,384]{2,1,0:T(8,128)(2,1)S(1)}, u32[]{:S(2)}, u32[]{:S(2)}) collective-permute-start(bf16[4,88,384]{2,1,0:T(8,128)(2,1)S(1)} %get-tuple-element.29), channel_id=1, source_target_pairs={{0,960},{1,65},{64,0},{65,129},{128,64},{129,193},{192,128},{193,2... | collective-permute-start | bytes 811016 | tf_op jit(solution)/shard_map/ppermute | solution.py:250
  88.5 0.7 collective-permute-done.2.far_ref
  89.1 8.5 %collective-permute-done.3.near_ref = bf16[4,88,384]{2,1,0:T(8,128)(2,1)S(1)} collective-permute-done((bf16[4,88,384]{2,1,0:T(8,128)(2,1)S(1)}, bf16[4,88,384]{2,1,0:T(8,128)(2,1)S(1)}, u32[]{:S(2)}, u32[]{:S(2)}) %collective-permute-start.3) | collective-permute-done | bytes 270368 | tf_op jit(solution)/shard_map/ppermute | solution.py:250
  97.6 0.0 collective-permute-done.4.back_ref
  97.6 0.1 stop.1
  97.8 1.9 %collective-permute-start.5 = (bf16[88,384]{1,0:T(8,128)(2,1)S(1)}, bf16[88,384]{1,0:T(8,128)(2,1)S(1)}, u32[]{:S(2)}, u32[]{:S(2)}) collective-permute-start(bf16[88,384]{1,0:T(8,128)(2,1)S(1)} %get-tuple-element.31), channel_id=1, source_target_pairs={{0,128},{1,897},{64,192},{65,961},{128,256},{129,1},{192,320},{193... | collective-permute-start | bytes 202760 | tf_op jit(solution)/shard_map/ppermute | solution.py:250
  99.7 7.8 %collective-permute-start.6 = (bf16[88,384]{1,0:T(8,128)(2,1)S(1)}, bf16[88,384]{1,0:T(8,128)(2,1)S(1)}, u32[]{:S(2)}, u32[]{:S(2)}) collective-permute-start(bf16[88,384]{1,0:T(8,128)(2,1)S(1)} %get-tuple-element.32), channel_id=1, source_target_pairs={{0,384},{1,641},{64,448},{65,705},{128,512},{129,769},{192,576},{1... | collective-permute-start | bytes 202760 | tf_op jit(solution)/shard_map/ppermute | solution.py:250
  107.5 4.9 %collective-permute-start.7 = (bf16[88,384]{1,0:T(8,128)(2,1)S(1)}, bf16[88,384]{1,0:T(8,128)(2,1)S(1)}, u32[]{:S(2)}, u32[]{:S(2)}) collective-permute-start(bf16[88,384]{1,0:T(8,128)(2,1)S(1)} %get-tuple-element.33), channel_id=1, source_target_pairs={{0,640},{1,385},{64,704},{65,449},{128,768},{129,513},{192,832},{1... | collective-permute-start | bytes 202760 | tf_op jit(solution)/shard_map/ppermute | solution.py:250
  112.5 4.8 %collective-permute-start.8 = (bf16[88,384]{1,0:T(8,128)(2,1)S(1)}, bf16[88,384]{1,0:T(8,128)(2,1)S(1)}, u32[]{:S(2)}, u32[]{:S(2)}) collective-permute-start(bf16[88,384]{1,0:T(8,128)(2,1)S(1)} %get-tuple-element.34), channel_id=1, source_target_pairs={{0,896},{1,129},{64,960},{65,193},{128,0},{129,257},{192,64},{193,... | collective-permute-start | bytes 202760 | tf_op jit(solution)/shard_map/ppermute | solution.py:250
  117.3 0.0 collective-permute-done.5.a_ref
  117.3 0.0 collective-permute-done.6.b_ref
  117.3 2.8 %collective-permute-done.7.c_ref = bf16[88,384]{1,0:T(8,128)(2,1)S(1)} collective-permute-done((bf16[88,384]{1,0:T(8,128)(2,1)S(1)}, bf16[88,384]{1,0:T(8,128)(2,1)S(1)}, u32[]{:S(2)}, u32[]{:S(2)}) %collective-permute-start.7) | collective-permute-done | bytes 67616 | tf_op jit(solution)/shard_map/ppermute | solution.py:250
  120.1 0.8 collective-permute-done.8.d_ref
  120.9 0.0 all-to-all-done.2.part_ref
  121.0 0.0 copy-done.3
  121.0 0.0 copy-done.4
  121.0 1.3 owner.1
  122.2 33.9 %all-gather.1.all_ref = bf16[16,85,384]{2,1,0:T(8,128)(2,1)S(1)} all-gather(bf16[1,85,384]{2,1,0:T(8,128)(2,1)S(1)} %bitcast.14), channel_id=2, replica_groups=mesh['rep'=16,'fs'=8,'tp_0'=4,'tp_1'=2] {'rep'}, dimensions={0}, use_global_device_ids=true | all-gather | bytes 1109760 | tf_op jit(solution)/shard_map/all_gather | solution.py:341
  156.1 1.5 out.1
  (1 shorter events, 0.0 us)
Async XLA Ops:
  23.1 27.3 %copy-start = (bf16[84,2048]{1,0:T(8,128)(2,1)S(1)}, bf16[84,2048]{1,0:T(8,128)(2,1)}, u32[]{:S(2)}) copy-start(bf16[84,2048]{1,0:T(8,128)(2,1)} %gate_w_ref.1) | copy-start | bytes 1032196
  23.1 27.3 %copy-start.1 = (bf16[84,2048]{1,0:T(8,128)(2,1)S(1)}, bf16[84,2048]{1,0:T(8,128)(2,1)}, u32[]{:S(2)}) copy-start(bf16[84,2048]{1,0:T(8,128)(2,1)} %up_w_ref.1) | copy-start | bytes 1032196
  23.1 27.3 %copy-start.2 = (bf16[84,2048]{1,0:T(8,128)(2,1)S(1)}, bf16[84,2048]{1,0:T(8,128)(2,1)}, u32[]{:S(2)}) copy-start(bf16[84,2048]{1,0:T(8,128)(2,1)} %down_w_ref.1) | copy-start | bytes 1032196
  23.2 27.3 %copy-start.5 = (f32[2048]{0:T(1024)S(1)}, f32[2048]{0:T(1024)}, u32[]{:S(2)}) copy-start(f32[2048]{0:T(1024)} %param.8) | copy-start | bytes 24580
  45.1 5.3 %collective-permute-start = (bf16[32,32,768]{2,1,0:T(8,128)(2,1)S(1)}, bf16[32,32,768]{2,1,0:T(8,128)(2,1)S(1)}, u32[]{:S(2)}, u32[]{:S(2)}) collective-permute-start(bf16[32,32,768]{2,1,0:T(8,128)(2,1)S(1)} %bitcast.8), channel_id=1, source_target_pairs={{0,1},{1,0},{2,3},{3,2},{4,5},{5,4},{6,7},{7,6},{8,9},{9,8},{10,11... | collective-permute-start | bytes 4718600 | tf_op jit(solution)/shard_map/ppermute | solution.py:268
  55.0 4.2 %collective-permute-start.1 = (bf16[33,32,384]{2,1,0:T(8,128)(2,1)S(1)}, bf16[33,32,384]{2,1,0:T(8,128)(2,1)S(1)}, u32[]{:S(2)}, u32[]{:S(2)}) collective-permute-start(bf16[33,32,384]{2,1,0:T(8,128)(2,1)S(1)} %get-tuple-element.24), channel_id=1, source_target_pairs={{0,1},{1,0},{2,3},{3,2},{4,5},{5,4},{6,7},{7,6},{8,9},{9,8},{10,11... | collective-permute-start | bytes 2433032 | tf_op jit(solution)/shard_map/ppermute | solution.py:306
  60.5 60.4 %copy-start.3 = (bf16[384,32]{0,1:T(8,128)(2,1)S(1)}, bf16[384,32]{0,1:T(8,128)(2,1)}, u32[]{:S(2)}) copy-start(bf16[384,32]{0,1:T(8,128)(2,1)} %param.7) | copy-start | bytes 73732
  60.5 60.4 %copy-start.4 = (bf16[384,32]{0,1:T(8,128)(2,1)S(1)}, bf16[384,32]{0,1:T(8,128)(2,1)}, u32[]{:S(2)}) copy-start(bf16[384,32]{0,1:T(8,128)(2,1)} %param.6) | copy-start | bytes 73732
  60.5 60.4 %all-to-all-start.2 = ((bf16[32,40,384]{2,1,0:T(8,128)(2,1)}), bf16[32,40,384]{2,1,0:T(8,128)(2,1)S(1)}, u32[]{:S(2)}, u32[]{:S(2)}) async-start(bf16[32,40,384]{2,1,0:T(8,128)(2,1)} %core.1), calls=%async_computation.2 | async-start | bytes 1966080 | tf_op jit(solution)/shard_map/all_to_all | solution.py:319
  66.4 22.8 %collective-permute-start.2 = (bf16[4,88,384]{2,1,0:T(8,128)(2,1)S(1)}, bf16[4,88,384]{2,1,0:T(8,128)(2,1)S(1)}, u32[]{:S(2)}, u32[]{:S(2)}) collective-permute-start(bf16[4,88,384]{2,1,0:T(8,128)(2,1)S(1)} %get-tuple-element.27), channel_id=1, source_target_pairs={{0,128},{1,897},{64,192},{65,961},{128,256},{129,1},{192,320},{193... | collective-permute-start | bytes 811016 | tf_op jit(solution)/shard_map/ppermute | solution.py:250
  72.5 25.1 %collective-permute-start.3 = (bf16[4,88,384]{2,1,0:T(8,128)(2,1)S(1)}, bf16[4,88,384]{2,1,0:T(8,128)(2,1)S(1)}, u32[]{:S(2)}, u32[]{:S(2)}) collective-permute-start(bf16[4,88,384]{2,1,0:T(8,128)(2,1)S(1)} %get-tuple-element.28), channel_id=1, source_target_pairs={{0,64},{1,961},{64,128},{65,1},{128,192},{129,65},{192,256},{193,1... | collective-permute-start | bytes 811016 | tf_op jit(solution)/shard_map/ppermute | solution.py:250
  76.8 20.8 %collective-permute-start.4 = (bf16[4,88,384]{2,1,0:T(8,128)(2,1)S(1)}, bf16[4,88,384]{2,1,0:T(8,128)(2,1)S(1)}, u32[]{:S(2)}, u32[]{:S(2)}) collective-permute-start(bf16[4,88,384]{2,1,0:T(8,128)(2,1)S(1)} %get-tuple-element.29), channel_id=1, source_target_pairs={{0,960},{1,65},{64,0},{65,129},{128,64},{129,193},{192,128},{193,2... | collective-permute-start | bytes 811016 | tf_op jit(solution)/shard_map/ppermute | solution.py:250
  97.8 19.5 %collective-permute-start.5 = (bf16[88,384]{1,0:T(8,128)(2,1)S(1)}, bf16[88,384]{1,0:T(8,128)(2,1)S(1)}, u32[]{:S(2)}, u32[]{:S(2)}) collective-permute-start(bf16[88,384]{1,0:T(8,128)(2,1)S(1)} %get-tuple-element.31), channel_id=1, source_target_pairs={{0,128},{1,897},{64,192},{65,961},{128,256},{129,1},{192,320},{193... | collective-permute-start | bytes 202760 | tf_op jit(solution)/shard_map/ppermute | solution.py:250
  99.7 17.6 %collective-permute-start.6 = (bf16[88,384]{1,0:T(8,128)(2,1)S(1)}, bf16[88,384]{1,0:T(8,128)(2,1)S(1)}, u32[]{:S(2)}, u32[]{:S(2)}) collective-permute-start(bf16[88,384]{1,0:T(8,128)(2,1)S(1)} %get-tuple-element.32), channel_id=1, source_target_pairs={{0,384},{1,641},{64,448},{65,705},{128,512},{129,769},{192,576},{1... | collective-permute-start | bytes 202760 | tf_op jit(solution)/shard_map/ppermute | solution.py:250
  107.5 12.6 %collective-permute-start.7 = (bf16[88,384]{1,0:T(8,128)(2,1)S(1)}, bf16[88,384]{1,0:T(8,128)(2,1)S(1)}, u32[]{:S(2)}, u32[]{:S(2)}) collective-permute-start(bf16[88,384]{1,0:T(8,128)(2,1)S(1)} %get-tuple-element.33), channel_id=1, source_target_pairs={{0,640},{1,385},{64,704},{65,449},{128,768},{129,513},{192,832},{1... | collective-permute-start | bytes 202760 | tf_op jit(solution)/shard_map/ppermute | solution.py:250
  112.5 8.5 %collective-permute-start.8 = (bf16[88,384]{1,0:T(8,128)(2,1)S(1)}, bf16[88,384]{1,0:T(8,128)(2,1)S(1)}, u32[]{:S(2)}, u32[]{:S(2)}) collective-permute-start(bf16[88,384]{1,0:T(8,128)(2,1)S(1)} %get-tuple-element.34), channel_id=1, source_target_pairs={{0,896},{1,129},{64,960},{65,193},{128,0},{129,257},{192,64},{193,... | collective-permute-start | bytes 202760 | tf_op jit(solution)/shard_map/ppermute | solution.py:250
where the time goes:
time: 158 us
  blocking collectives  77.4 us (49%)
  starting transfers between devices  51.3 us (32%)
  waiting for transfers between devices  18.3 us (12%)
  Pallas kernels  8.76 us (6%)
    all_to_all x2, blocking collectives, spread(): return lax.all_to_all(copies, axis, 0, 0, tiled=True)  43.5 us
    ppermute x7, starting transfers between devices, shifted(): return lax.ppermute(v, ('rep', 'tp_1'), pairs)  41.6 us
    all_gather x1, blocking collectives, body(): everything = lax.all_gather(chunk, 'rep', axis=0, tiled=False)  33.9 us
    ppermute x7, waiting for transfers between devices, shifted(): return lax.ppermute(v, ('rep', 'tp_1'), pairs)  12.8 us
    all_to_all x1, starting transfers between devices, body(): parts = lax.all_to_all(ready, FS_TP[:2], 0, 0, tiled=True)  5.83 us
    pallas_call x1, Pallas kernels, body(): pl.pallas_call(functools.partial(main_kernel, sizes), out_shape=[shape(pe...  4.56 us
    ppermute x1, waiting for transfers between devices, body(): other = lax.ppermute(plane, 'tp_1', [(0, 1), (1, 0)])  3.38 us
  transfers between devices with their start and end apart: 10, of which 6 were waited for; matrix products, arithmetic and copies ran while one was open for 0% of the time, Pallas kernels for 0%

commit v1 on v0

--- a/solution.py
+++ b/solution.py
@@ -15,6 +15,7 @@
 F32 = jnp.float32
 LANES = 128
 VMEM = pl.BlockSpec(memory_space=pltpu.VMEM)
+ANY = pl.BlockSpec(memory_space=pl.ANY)
 
 
 def gain_columns(gain_ref, out_ref):
@@ -28,14 +29,44 @@
     return high, (v - high.astype(F32)).astype(BF)
 
 
+def square_sum(ref, tokens):
+    slabs, block, _ = ref.shape
+
+    def step(s, acc):
+        v = ref[s, :, 0:tokens].astype(F32)
+        v = v * v
+        parts = [v[8 * k : 8 * k + 8, :] for k in range(block // 8)]
+        while len(parts) > 1:
+            parts = [a + b for a, b in zip(parts[::2], parts[1::2])]
+        return acc + parts[0]
+
+    return lax.fori_loop(0, slabs, step, jnp.zeros((8, tokens), F32), unroll=4)
+
+
+def ready_kernel(
+    tokens, own_ref, gate_w_ref, up_w_ref, down_w_ref, gain_ref, pair_ref, down_ref, columns_ref, square_ref
+):
+    hidden, width = gate_w_ref.shape
+    padded = down_ref.shape[0]
+    low = padded - 16
+    pair_ref[low:padded, :] = jnp.zeros((16, width), BF)
+    pair_ref[padded + low : 2 * padded, :] = jnp.zeros((16, width), BF)
+    down_ref[low:padded, :] = jnp.zeros((16, width), BF)
+    pair_ref[0:hidden, :] = gate_w_ref[...]
+    pair_ref[padded : padded + hidden, :] = up_w_ref[...]
+    down_ref[0:hidden, :] = down_w_ref[...]
+    gain_columns(gain_ref, columns_ref)
+    square_ref[...] = square_sum(own_ref, tokens)
+
+
 def main_kernel(
     sizes,
     own_ref,
     other_ref,
-    gate_w_ref,
-    up_w_ref,
-    down_w_ref,
-    gain_ref,
+    pair_s,
+    down_s,
+    gain_s,
+    square_ref,
     keep_ref,
     send_ref,
     row_ref,
@@ -46,44 +77,23 @@
     stay_ref,
     normed_s,
     cot_s,
-    pair_s,
-    down_s,
     delta_s,
     hidden_s,
-    gain_s,
     part_s,
     grad_s,
 ):
-    n_rep, n_fs, n_x, n_core, tokens, hidden, padded, width, block = sizes
+    n_rep, n_fs, n_x, n_core, tokens, _, padded, width, block = sizes
     core = lax.axis_index("tp_1")
     z = lax.axis_index("rep")
     tall = grad_s.shape[1]
-
-    low = padded - 16
-    pair_s[low:padded, :] = jnp.zeros((16, width), BF)
-    pair_s[padded + low : 2 * padded, :] = jnp.zeros((16, width), BF)
-    down_s[low:padded, :] = jnp.zeros((16, width), BF)
-    pair_s[0:hidden, :] = gate_w_ref[...]
-    pair_s[padded : padded + hidden, :] = up_w_ref[...]
-    down_s[0:hidden, :] = down_w_ref[...]
-    gain_columns(gain_ref, gain_s)
-
-    def square_sum(s, acc):
-        for ref in (own_ref, other_ref):
-            v = ref[s, :, 0:tokens].astype(F32)
-            v = v * v
-            for k in range(block // 8):
-                acc = acc + v[8 * k : 8 * k + 8, :]
-        return acc
-
-    total = lax.fori_loop(0, n_fs * n_x, square_sum, jnp.zeros((8, tokens), F32))
+    total = square_ref[...] + square_sum(other_ref, tokens)
     mean = jnp.sum(total, axis=0, keepdims=True) / width
     inv = lax.rsqrt(mean + EPS)
     inv_ref[...] = jnp.broadcast_to(inv, (8, tokens))
 
     def normalise(s, carry):
-        x = s // n_fs
-        y = s % n_fs
+        x = n_x - 1 - s // n_fs
+        y = n_fs - 1 - s % n_fs
         for ref, which in ((own_ref, core), (other_ref, 1 - core)):
             at = pl.multiple_of(((y * n_x + x) * n_core + which) * block, block)
             v = ref[s, :, 0:tokens].astype(F32) * inv
@@ -127,8 +137,9 @@
         send_ref[s] = part_s[n_core * s + 1 - core]
         return carry
 
-    lax.fori_loop(0, n_fs * n_x, share, 0)
-
+    lax.fori_loop(0, n_fs * n_x, share, 0, unroll=4)
+
+    side = 1 - 2 * core
     for b in range(width // step):
         rows = slice(b * step, (b + 1) * step)
         two = lax.dot_general(
@@ -140,37 +151,47 @@
         for k in range(step // LANES):
             at = b * (step // LANES) + k
             lanes = slice(k * LANES, (k + 1) * LANES)
-            grad_s[at, :, 0:LANES] = two[0:tall, lanes]
-            grad_s[at, :, LANES : 2 * LANES] = two[padded : padded + tall, lanes]
-            grad_s[at, :, 2 * LANES : 3 * LANES] = one[0:tall, lanes]
-
-    side = 1 - 2 * core
+            grad_s[at, :, 0:LANES] = two[0:tall, lanes].astype(BF)
+            grad_s[at, :, LANES : 2 * LANES] = two[padded : padded + tall, lanes].astype(BF)
+            grad_s[at, :, 2 * LANES : 3 * LANES] = one[0:tall, lanes].astype(BF)
+
     for i in range(4):
         for ref, base in ((far_ref, 4), (near_ref, 3), (back_ref, 1), (stay_ref, 2)):
-            chunk = lax.rem(z + side * (base + 4 * i) + 2 * n_rep, n_rep)
-            ref[i] = grad_s[chunk].astype(ref.dtype)
-
-
-def core_kernel(block, keep_ref, got_ref, row_ref, out_ref):
-    slabs = keep_ref.shape[0]
-    tokens = keep_ref.shape[2]
+            ref[i] = grad_s[lax.rem(z + side * (base + 4 * i) + 2 * n_rep, n_rep)]
+
+
+def core_kernel(block, keep_ref, got_ref, row_ref, out_ref, slab_s, sems):
+    slabs = got_ref.shape[0] - 1
+    groups = got_ref.shape[2] // LANES
+    pieces = sems.shape[0]
+    each = slabs // pieces
     other = got_ref[slabs, 0:8, :].astype(F32)
     row = row_ref[0:1, :] + other[0:1, :] + other[1:2, :]
     high, low_part = split_in_two(row)
-    tail = jnp.concatenate([high, low_part, jnp.zeros((6, tokens), BF)], axis=0)
+    tail = [v[:, k * LANES : (k + 1) * LANES] for v in (high, low_part) for k in range(groups)]
+    tail = jnp.concatenate(tail + [jnp.zeros((8 - 2 * groups, LANES), BF)], axis=0)
 
     def add(s, carry):
-        v = keep_ref[s].astype(F32) + got_ref[s].astype(F32)
-        out_ref[s, 0:block, :] = v.astype(BF)
-        out_ref[s, block : block + 8, :] = tail
+        v = (keep_ref[s].astype(F32) + got_ref[s].astype(F32)).astype(BF)
+        for k in range(groups):
+            slab_s[s, k * block : (k + 1) * block, :] = v[:, k * LANES : (k + 1) * LANES]
+        slab_s[s, groups * block : groups * block + 8, :] = tail
         return carry
 
-    lax.fori_loop(0, slabs, add, 0)
+    copies = []
+    for p in range(pieces):
+        lax.fori_loop(p * each, (p + 1) * each, add, 0, unroll=4)
+        here = pl.ds(p * each, each)
+        copies.append(pltpu.make_async_copy(slab_s.at[here], out_ref.at[here], sems.at[p]))
+        copies[-1].start()
+    for copy in copies:
+        copy.wait()
 
 
 def stop_kernel(far_ref, near_ref, back_ref, stay_ref, *out_refs):
     for i, out_ref in enumerate(out_refs):
-        v = stay_ref[i] + far_ref[i].astype(F32) + near_ref[i].astype(F32) + back_ref[i].astype(F32)
+        v = stay_ref[i].astype(F32) + far_ref[i].astype(F32)
+        v = v + near_ref[i].astype(F32) + back_ref[i].astype(F32)
         out_ref[...] = v.astype(BF)
 
 
@@ -187,22 +208,28 @@
     d_ref,
     input_ref,
     chunk_ref,
-    gain_s,
+    column_s,
 ):
     n_x, n_core, width, hidden, block = sizes
-    sources, rows, tokens = part_ref.shape
-    me = (lax.axis_index("fs") * n_x + lax.axis_index("tp_0")) * n_core + lax.axis_index("tp_1")
-    gain_columns(gain_ref, gain_s)
+    sources, rows, _ = part_ref.shape
+    tokens = tok_ref.shape[1]
+    groups = tokens // LANES
 
     def add(s, acc):
         return acc + part_ref[s].astype(F32)
 
-    total = lax.fori_loop(0, sources, add, jnp.zeros((rows, tokens), F32))
-    summed = total[0:block, :]
-    row = (total[block : block + 1, :] + total[block + 1 : block + 2, :]) / width
+    total = lax.fori_loop(0, sources, add, jnp.zeros((rows, LANES), F32), unroll=4)
+    summed = jnp.concatenate([total[k * block : (k + 1) * block, :] for k in range(groups)], axis=1)
+    at = groups * block
+    row = [total[at + k : at + k + 1, :] + total[at + groups + k : at + groups + k + 1, :] for k in range(groups)]
+    row = jnp.concatenate(row, axis=1) / width
+    me = (lax.axis_index("fs") * n_x + lax.axis_index("tp_0")) * n_core + lax.axis_index("tp_1")
+    per = LANES // block
+    mine = gain_ref[pl.ds(lax.div(me, per), 1), :]
+    column_s[...] = jnp.broadcast_to(mine, (LANES, LANES)).T
+    g = column_s[pl.ds(pl.multiple_of(lax.rem(me, per) * block, block), block), :]
     inv = inv_ref[0:1, :]
-    g = gain_s[pl.ds(pl.multiple_of(me * block, block), block), :]
-    d_unit = summed * jnp.concatenate([g] * (tokens // LANES), axis=1)
+    d_unit = summed * jnp.concatenate([g] * groups, axis=1)
     unit = tok_ref[...].astype(F32) * inv
     input_ref[...] = (cot_ref[...].astype(F32) + inv * (d_unit - unit * row)).astype(BF)
 
@@ -220,9 +247,10 @@
     chunk_ref[...] = chunk[0 : hidden + 1, :].astype(BF)
 
 
-def out_kernel(all_ref, gate_ref, up_ref, down_ref, gain_ref):
+def out_kernel(all_ref, made_ref, gate_ref, up_ref, down_ref, gain_ref, input_ref):
     n, tall, _ = all_ref.shape
     hidden = tall - 1
+    input_ref[...] = made_ref[...]
     total = jnp.zeros((1, 3 * LANES), F32)
     for b in range(n):
         lanes = slice(b * LANES, (b + 1) * LANES)
@@ -238,7 +266,8 @@
 def spread(block, axis):
     n = lax.axis_size(axis)
     copies = jnp.broadcast_to(block[None], (n,) + block.shape)
-    return lax.all_to_all(copies, axis, 0, 0, tiled=True)
+    backwards = [list(range(n - 1, -1, -1))]
+    return lax.all_to_all(copies, axis, 0, 0, tiled=True, axis_index_groups=backwards)
 
 
 def shifted(v, by):
@@ -271,6 +300,21 @@
     def shape(*dims, dtype=BF):
         return jax.ShapeDtypeStruct(dims, dtype)
 
+    pair, down, columns, square = pl.pallas_call(
+        functools.partial(ready_kernel, rows),
+        out_shape=[
+            shape(2 * padded, width),
+            shape(padded, width),
+            shape(width, LANES, dtype=F32),
+            shape(8, rows, dtype=F32),
+        ],
+        in_specs=[VMEM] * 5,
+        out_specs=[VMEM] * 4,
+        compiler_params=pltpu.CompilerParams(vmem_limit_bytes=8 * 2**20),
+        cost_estimate=pl.CostEstimate(flops=10**7, bytes_accessed=4 * 10**6, transcendentals=0),
+        name="ready",
+    )(plane, w_gate, w_up, w_down, gain_rows)
+
     sizes = (n_rep, n_fs, n_x, n_core, rows, hidden, padded, width, block)
     group = (4, tall, 3 * LANES)
     keep, send, row, inv, far, near, back, stay = pl.pallas_call(
@@ -283,25 +327,22 @@
             shape(*group),
             shape(*group),
             shape(*group),
-            shape(*group, dtype=F32),
+            shape(*group),
         ],
         in_specs=[VMEM] * 6,
         out_specs=[VMEM] * 8,
         scratch_shapes=[
             pltpu.VMEM((width, rows), BF),
             pltpu.VMEM((width, rows), BF),
-            pltpu.VMEM((2 * padded, width), BF),
-            pltpu.VMEM((padded, width), BF),
             pltpu.VMEM((2 * padded, rows), BF),
             pltpu.VMEM((padded, rows), BF),
-            pltpu.VMEM((width, LANES), F32),
             pltpu.VMEM((peers * n_core, block, rows), BF),
-            pltpu.VMEM((n_blocks, tall, 3 * LANES), F32),
+            pltpu.VMEM((n_blocks, tall, 3 * LANES), BF),
         ],
         compiler_params=pltpu.CompilerParams(vmem_limit_bytes=34 * 2**20),
         cost_estimate=pl.CostEstimate(flops=11 * 10**8, bytes_accessed=10**7, transcendentals=0),
         name="main",
-    )(plane, other, w_gate, w_up, w_down, gain_rows)
+    )(plane, other, pair, down, columns, square)
 
     got = lax.ppermute(send, "tp_1", [(0, 1), (1, 0)])
     far = shifted(far, 2)
@@ -309,9 +350,13 @@
     back = shifted(back, -1)
     ready = pl.pallas_call(
         functools.partial(core_kernel, block),
-        out_shape=shape(peers, block + 8, rows),
+        out_shape=shape(peers, block * (rows // LANES) + 8, LANES),
         in_specs=[VMEM] * 3,
-        out_specs=VMEM,
+        out_specs=ANY,
+        scratch_shapes=[
+            pltpu.VMEM((peers, block * (rows // LANES) + 8, LANES), BF),
+            pltpu.SemaphoreType.DMA((4,)),
+        ],
         compiler_params=pltpu.CompilerParams(vmem_limit_bytes=8 * 2**20),
         cost_estimate=pl.CostEstimate(flops=10**6, bytes_accessed=3 * 10**6, transcendentals=0),
         name="core",
@@ -326,27 +371,31 @@
         cost_estimate=pl.CostEstimate(flops=10**6, bytes_accessed=2 * 10**6, transcendentals=0),
         name="stop",
     )(far, near, back, stay)
-    sums = [shifted(s, by) for s, by in zip(sums, (2, 6, -6, -2))]
-
-    grad_input, chunk = pl.pallas_call(
+    moved = []
+    for k, by in enumerate((2, 6, -6, -2)):
+        moved.append(shifted(sums[k], by))
+    sums = moved
+
+    made, chunk = pl.pallas_call(
         functools.partial(owner_kernel, (n_x, n_core, width, hidden, block)),
         out_shape=[shape(block, rows), shape(hidden + 1, 3 * LANES)],
         in_specs=[VMEM] * 9,
         out_specs=[VMEM] * 2,
-        scratch_shapes=[pltpu.VMEM((width, LANES), F32)],
+        scratch_shapes=[pltpu.VMEM((LANES, LANES), F32)],
         compiler_params=pltpu.CompilerParams(vmem_limit_bytes=12 * 2**20),
         cost_estimate=pl.CostEstimate(flops=10**8, bytes_accessed=2 * 10**6, transcendentals=0),
         name="owner",
     )(parts, tok_t, cot_t, inv, gain_rows, *sums)
     everything = lax.all_gather(chunk, "rep", axis=0, tiled=False)
-    grad_gate, grad_up, grad_down, grad_gain = pl.pallas_call(
+    grad_gate, grad_up, grad_down, grad_gain, grad_input = pl.pallas_call(
         out_kernel,
-        out_shape=[shape(hidden, width, dtype=F32)] * 3 + [shape(1, block, dtype=F32)],
-        in_specs=[VMEM],
-        out_specs=[VMEM] * 4,
+        out_shape=[shape(hidden, width, dtype=F32)] * 3
+        + [shape(1, block, dtype=F32), shape(block, rows)],
+        in_specs=[VMEM] * 2,
+        out_specs=[VMEM] * 5,
         compiler_params=pltpu.CompilerParams(vmem_limit_bytes=12 * 2**20),
         name="out",
-    )(everything)
+    )(everything, made)
     return (grad_input.T, grad_gain.reshape(block), grad_gate, grad_up, grad_down)
 
 

time: 158 us -> 156 us (0.987)
  blocking collectives: 77.4 us -> 74.3 us
  starting transfers between devices: 51.3 us -> 54.1 us
    all_to_all x2, blocking collectives: 43.5 us -> 39.9 us  [spread(): lax.all_to_all(copies, axis, 0, 0, tiled=True, axis_index_groups=backwards)]
    all_to_all x1, starting transfers between devices: 5.83 us -> 8.57 us  [body(): parts = lax.all_to_all(ready, FS_TP[:2], 0, 0, tiled=True)]
where the time goes in v1:
time: 156 us; the launch traced here: 155 us
  blocking collectives  74.3 us (48%)
  starting transfers between devices  54.1 us (35%)
  waiting for transfers between devices  17.8 us (11%)
  Pallas kernels  7.31 us (5%)
    ppermute x7, starting transfers between devices, shifted(): return lax.ppermute(v, ('rep', 'tp_1'), pairs)  41.6 us
    all_to_all x2, blocking collectives, spread(): lax.all_to_all(copies, axis, 0, 0, tiled=True, axis_index_groups=backwards)  39.9 us
    all_gather x1, blocking collectives, body(): everything = lax.all_gather(chunk, 'rep', axis=0, tiled=False)  34.3 us
    ppermute x7, waiting for transfers between devices, shifted(): return lax.ppermute(v, ('rep', 'tp_1'), pairs)  12.8 us
    all_to_all x1, starting transfers between devices, body(): parts = lax.all_to_all(ready, FS_TP[:2], 0, 0, tiled=True)  8.57 us
    pallas_call x1, Pallas kernels, body(): pl.pallas_call(functools.partial(main_kernel, sizes), out_shape=[shape(pe...  3.83 us
  transfers between devices with their start and end apart: 10, of which 6 were waited for; matrix products, arithmetic and copies ran while one was open for 0% of the time, Pallas kernels for 0%

profile of v1, /device:TPU:6, one launch (start us, length us, event | category | flops | bytes accessed | tf_op | source)
XLA Modules:
  0.0 155.2 jit_solution(13699531655101750426)
XLA Ops:
  0.6 0.8 pad_maximum_fusion
  1.4 18.1 %all_to_all.15 = bf16[8,32,768]{2,1,0:T(8,128)(2,1)S(1)} all-to-all(bf16[8,32,768]{2,1,0:T(8,128)(2,1)S(1)} %broadcast_in_dim.6), channel_id=1, replica_groups={{56,48,40,32,24,16,8,0},{57,49,41,33,25,17,9,1},{58,50,42,34,26,18,10,2..., dimensions={0} | all-to-all | bytes 786432 | tf_op jit(solution)/shard_map/all_to_all | solution.py:270
  19.5 0.1 broadcast_in_dim.15
  19.6 0.0 copy-start
  19.6 0.0 copy-start.1
  19.6 0.0 copy-start.2
  19.6 0.0 copy-start.5
  19.7 21.9 %all_to_all.16 = bf16[4,256,768]{2,1,0:T(8,128)(2,1)S(1)} all-to-all(bf16[4,256,768]{2,1,0:T(8,128)(2,1)S(1)} %broadcast_in_dim.15), channel_id=1, replica_groups={{6,4,2,0},{7,5,3,1},{14,12,10,8},{15,13,11,9},{22,20,18,16},{23,21,19,1..., dimensions={0} | all-to-all | bytes 3145728 | tf_op jit(solution)/shard_map/all_to_all | solution.py:270
  41.5 1.9 %collective-permute-start = (bf16[32,32,768]{2,1,0:T(8,128)(2,1)S(1)}, bf16[32,32,768]{2,1,0:T(8,128)(2,1)S(1)}, u32[]{:S(2)}, u32[]{:S(2)}) collective-permute-start(bf16[32,32,768]{2,1,0:T(8,128)(2,1)S(1)} %bitcast.8), channel_id=1, source_target_pairs={{0,1},{1,0},{2,3},{3,2},{4,5},{5,4},{6,7},{7,6},{8,9},{9,8},{10,11... | collective-permute-start | bytes 4718600 | tf_op jit(solution)/shard_map/ppermute | solution.py:297
  43.4 0.0 copy-done
  43.5 0.0 copy-done.1
  43.5 0.0 copy-done.2
  43.5 0.0 copy-done.5
  43.5 0.5 ready.1
  44.0 2.8 %collective-permute-done.other_ref = bf16[32,32,768]{2,1,0:T(8,128)(2,1)S(1)} collective-permute-done((bf16[32,32,768]{2,1,0:T(8,128)(2,1)S(1)}, bf16[32,32,768]{2,1,0:T(8,128)(2,1)S(1)}, u32[]{:S(2)}, u32[]{:S(2)}) %collective-permute-start) | collective-permute-done | bytes 1572896 | tf_op jit(solution)/shard_map/ppermute | solution.py:297
  46.8 3.8 %main.1 = (bf16[32,32,384]{2,1,0:T(8,128)(2,1)S(1)}, bf16[33,32,384]{2,1,0:T(8,128)(2,1)S(1)}, f32[8,384]{1,0:T(8,128)S(1)}, f32[8,384]{1,0:T(8,128)S(1)}, bf16[...) custom-call(bf16[32,32,768]{2,1,0:T(8,128)(2,1)S(1)} %bitcast.10, ...), custom_call_target="tpu_custom_call" | custom-call | flops 1100000000 | bytes 10000000 | tf_op jit(solution)/shard_map/main/pallas_call | solution.py:320
  50.7 2.0 %collective-permute-start.1 = (bf16[33,32,384]{2,1,0:T(8,128)(2,1)S(1)}, bf16[33,32,384]{2,1,0:T(8,128)(2,1)S(1)}, u32[]{:S(2)}, u32[]{:S(2)}) collective-permute-start(bf16[33,32,384]{2,1,0:T(8,128)(2,1)S(1)} %get-tuple-element.33), channel_id=1, source_target_pairs={{0,1},{1,0},{2,3},{3,2},{4,5},{5,4},{6,7},{7,6},{8,9},{9,8},{10,11... | collective-permute-start | bytes 2433032 | tf_op jit(solution)/shard_map/ppermute | solution.py:347
  52.7 2.2 %collective-permute-done.1.got_ref = bf16[33,32,384]{2,1,0:T(8,128)(2,1)S(1)} collective-permute-done((bf16[33,32,384]{2,1,0:T(8,128)(2,1)S(1)}, bf16[33,32,384]{2,1,0:T(8,128)(2,1)S(1)}, u32[]{:S(2)}, u32[]{:S(2)}) %collective-permute-start.1) | collective-permute-done | bytes 811040 | tf_op jit(solution)/shard_map/ppermute | solution.py:347
  54.9 1.0 core.1
  55.9 0.0 copy-start.3
  55.9 0.0 copy-start.4
  55.9 8.6 %all-to-all-start.2 = ((bf16[32,104,128]{2,1,0:T(8,128)(2,1)}), bf16[32,104,128]{2,1,0:T(8,128)(2,1)S(1)}, u32[]{:S(2)}, u32[]{:S(2)}) async-start(bf16[32,104,128]{2,1,0:T(8,128)(2,1)} %core.1), calls=%async_computation.2 | async-start | bytes 1703936 | tf_op jit(solution)/shard_map/all_to_all | solution.py:364
  64.5 6.1 %collective-permute-start.2 = (bf16[4,88,384]{2,1,0:T(8,128)(2,1)S(1)}, bf16[4,88,384]{2,1,0:T(8,128)(2,1)S(1)}, u32[]{:S(2)}, u32[]{:S(2)}) collective-permute-start(bf16[4,88,384]{2,1,0:T(8,128)(2,1)S(1)} %get-tuple-element.36), channel_id=1, source_target_pairs={{0,128},{1,897},{64,192},{65,961},{128,256},{129,1},{192,320},{193... | collective-permute-start | bytes 811016 | tf_op jit(solution)/shard_map/ppermute | solution.py:279
  70.6 4.3 %collective-permute-start.3 = (bf16[4,88,384]{2,1,0:T(8,128)(2,1)S(1)}, bf16[4,88,384]{2,1,0:T(8,128)(2,1)S(1)}, u32[]{:S(2)}, u32[]{:S(2)}) collective-permute-start(bf16[4,88,384]{2,1,0:T(8,128)(2,1)S(1)} %get-tuple-element.37), channel_id=1, source_target_pairs={{0,64},{1,961},{64,128},{65,1},{128,192},{129,65},{192,256},{193,1... | collective-permute-start | bytes 811016 | tf_op jit(solution)/shard_map/ppermute | solution.py:279
  74.9 11.7 %collective-permute-start.4 = (bf16[4,88,384]{2,1,0:T(8,128)(2,1)S(1)}, bf16[4,88,384]{2,1,0:T(8,128)(2,1)S(1)}, u32[]{:S(2)}, u32[]{:S(2)}) collective-permute-start(bf16[4,88,384]{2,1,0:T(8,128)(2,1)S(1)} %get-tuple-element.38), channel_id=1, source_target_pairs={{0,960},{1,65},{64,0},{65,129},{128,64},{129,193},{192,128},{193,2... | collective-permute-start | bytes 811016 | tf_op jit(solution)/shard_map/ppermute | solution.py:279
  86.6 0.7 collective-permute-done.2.far_ref
  87.2 8.6 %collective-permute-done.3.near_ref = bf16[4,88,384]{2,1,0:T(8,128)(2,1)S(1)} collective-permute-done((bf16[4,88,384]{2,1,0:T(8,128)(2,1)S(1)}, bf16[4,88,384]{2,1,0:T(8,128)(2,1)S(1)}, u32[]{:S(2)}, u32[]{:S(2)}) %collective-permute-start.3) | collective-permute-done | bytes 270368 | tf_op jit(solution)/shard_map/ppermute | solution.py:279
  95.8 0.0 collective-permute-done.4.back_ref
  95.8 0.1 stop.1
  96.0 1.9 %collective-permute-start.5 = (bf16[88,384]{1,0:T(8,128)(2,1)S(1)}, bf16[88,384]{1,0:T(8,128)(2,1)S(1)}, u32[]{:S(2)}, u32[]{:S(2)}) collective-permute-start(bf16[88,384]{1,0:T(8,128)(2,1)S(1)} %get-tuple-element.40), channel_id=1, source_target_pairs={{0,128},{1,897},{64,192},{65,961},{128,256},{129,1},{192,320},{193... | collective-permute-start | bytes 202760 | tf_op jit(solution)/shard_map/ppermute | solution.py:279
  97.9 7.7 %collective-permute-start.6 = (bf16[88,384]{1,0:T(8,128)(2,1)S(1)}, bf16[88,384]{1,0:T(8,128)(2,1)S(1)}, u32[]{:S(2)}, u32[]{:S(2)}) collective-permute-start(bf16[88,384]{1,0:T(8,128)(2,1)S(1)} %get-tuple-element.41), channel_id=1, source_target_pairs={{0,384},{1,641},{64,448},{65,705},{128,512},{129,769},{192,576},{1... | collective-permute-start | bytes 202760 | tf_op jit(solution)/shard_map/ppermute | solution.py:279
  105.7 5.0 %collective-permute-start.7 = (bf16[88,384]{1,0:T(8,128)(2,1)S(1)}, bf16[88,384]{1,0:T(8,128)(2,1)S(1)}, u32[]{:S(2)}, u32[]{:S(2)}) collective-permute-start(bf16[88,384]{1,0:T(8,128)(2,1)S(1)} %get-tuple-element.42), channel_id=1, source_target_pairs={{0,640},{1,385},{64,704},{65,449},{128,768},{129,513},{192,832},{1... | collective-permute-start | bytes 202760 | tf_op jit(solution)/shard_map/ppermute | solution.py:279
  110.7 4.8 %collective-permute-start.8 = (bf16[88,384]{1,0:T(8,128)(2,1)S(1)}, bf16[88,384]{1,0:T(8,128)(2,1)S(1)}, u32[]{:S(2)}, u32[]{:S(2)}) collective-permute-start(bf16[88,384]{1,0:T(8,128)(2,1)S(1)} %get-tuple-element.43), channel_id=1, source_target_pairs={{0,896},{1,129},{64,960},{65,193},{128,0},{129,257},{192,64},{193,... | collective-permute-start | bytes 202760 | tf_op jit(solution)/shard_map/ppermute | solution.py:279
  115.5 0.0 collective-permute-done.5.a_ref
  115.5 0.0 collective-permute-done.6.b_ref
  115.5 2.7 %collective-permute-done.7.c_ref = bf16[88,384]{1,0:T(8,128)(2,1)S(1)} collective-permute-done((bf16[88,384]{1,0:T(8,128)(2,1)S(1)}, bf16[88,384]{1,0:T(8,128)(2,1)S(1)}, u32[]{:S(2)}, u32[]{:S(2)}) %collective-permute-start.7) | collective-permute-done | bytes 67616 | tf_op jit(solution)/shard_map/ppermute | solution.py:279
  118.3 0.8 collective-permute-done.8.d_ref
  119.1 0.0 all-to-all-done.2.part_ref
  119.1 0.0 copy-done.3
  119.1 0.0 copy-done.4
  119.1 0.3 owner.1
  119.4 34.3 %all-gather.1.all_ref = bf16[16,85,384]{2,1,0:T(8,128)(2,1)S(1)} all-gather(bf16[1,85,384]{2,1,0:T(8,128)(2,1)S(1)} %bitcast.15), channel_id=2, replica_groups=mesh['rep'=16,'fs'=8,'tp_0'=4,'tp_1'=2] {'rep'}, dimensions={0}, use_global_device_ids=true | all-gather | bytes 1109760 | tf_op jit(solution)/shard_map/all_gather | solution.py:389
  153.7 1.5 out.1
  (1 shorter events, 0.0 us)
Async XLA Ops:
  19.6 23.8 %copy-start = (bf16[84,2048]{1,0:T(8,128)(2,1)S(1)}, bf16[84,2048]{1,0:T(8,128)(2,1)}, u32[]{:S(2)}) copy-start(bf16[84,2048]{1,0:T(8,128)(2,1)} %gate_w_ref.1) | copy-start | bytes 1032196
  19.6 23.8 %copy-start.1 = (bf16[84,2048]{1,0:T(8,128)(2,1)S(1)}, bf16[84,2048]{1,0:T(8,128)(2,1)}, u32[]{:S(2)}) copy-start(bf16[84,2048]{1,0:T(8,128)(2,1)} %up_w_ref.1) | copy-start | bytes 1032196
  19.6 23.8 %copy-start.2 = (bf16[84,2048]{1,0:T(8,128)(2,1)S(1)}, bf16[84,2048]{1,0:T(8,128)(2,1)}, u32[]{:S(2)}) copy-start(bf16[84,2048]{1,0:T(8,128)(2,1)} %down_w_ref.1) | copy-start | bytes 1032196
  19.6 23.8 %copy-start.5 = (f32[2048]{0:T(1024)S(1)}, f32[2048]{0:T(1024)}, u32[]{:S(2)}) copy-start(f32[2048]{0:T(1024)} %param.8) | copy-start | bytes 24580
  41.5 5.3 %collective-permute-start = (bf16[32,32,768]{2,1,0:T(8,128)(2,1)S(1)}, bf16[32,32,768]{2,1,0:T(8,128)(2,1)S(1)}, u32[]{:S(2)}, u32[]{:S(2)}) collective-permute-start(bf16[32,32,768]{2,1,0:T(8,128)(2,1)S(1)} %bitcast.8), channel_id=1, source_target_pairs={{0,1},{1,0},{2,3},{3,2},{4,5},{5,4},{6,7},{7,6},{8,9},{9,8},{10,11... | collective-permute-start | bytes 4718600 | tf_op jit(solution)/shard_map/ppermute | solution.py:297
  50.7 4.2 %collective-permute-start.1 = (bf16[33,32,384]{2,1,0:T(8,128)(2,1)S(1)}, bf16[33,32,384]{2,1,0:T(8,128)(2,1)S(1)}, u32[]{:S(2)}, u32[]{:S(2)}) collective-permute-start(bf16[33,32,384]{2,1,0:T(8,128)(2,1)S(1)} %get-tuple-element.33), channel_id=1, source_target_pairs={{0,1},{1,0},{2,3},{3,2},{4,5},{5,4},{6,7},{7,6},{8,9},{9,8},{10,11... | collective-permute-start | bytes 2433032 | tf_op jit(solution)/shard_map/ppermute | solution.py:347
  55.9 63.2 %copy-start.3 = (bf16[384,32]{0,1:T(8,128)(2,1)S(1)}, bf16[384,32]{0,1:T(8,128)(2,1)}, u32[]{:S(2)}) copy-start(bf16[384,32]{0,1:T(8,128)(2,1)} %param.7) | copy-start | bytes 73732
  55.9 63.2 %copy-start.4 = (bf16[384,32]{0,1:T(8,128)(2,1)S(1)}, bf16[384,32]{0,1:T(8,128)(2,1)}, u32[]{:S(2)}) copy-start(bf16[384,32]{0,1:T(8,128)(2,1)} %param.6) | copy-start | bytes 73732
  55.9 63.1 %all-to-all-start.2 = ((bf16[32,104,128]{2,1,0:T(8,128)(2,1)}), bf16[32,104,128]{2,1,0:T(8,128)(2,1)S(1)}, u32[]{:S(2)}, u32[]{:S(2)}) async-start(bf16[32,104,128]{2,1,0:T(8,128)(2,1)} %core.1), calls=%async_computation.2 | async-start | bytes 1703936 | tf_op jit(solution)/shard_map/all_to_all | solution.py:364
  64.5 22.7 %collective-permute-start.2 = (bf16[4,88,384]{2,1,0:T(8,128)(2,1)S(1)}, bf16[4,88,384]{2,1,0:T(8,128)(2,1)S(1)}, u32[]{:S(2)}, u32[]{:S(2)}) collective-permute-start(bf16[4,88,384]{2,1,0:T(8,128)(2,1)S(1)} %get-tuple-element.36), channel_id=1, source_target_pairs={{0,128},{1,897},{64,192},{65,961},{128,256},{129,1},{192,320},{193... | collective-permute-start | bytes 811016 | tf_op jit(solution)/shard_map/ppermute | solution.py:279
  70.6 25.2 %collective-permute-start.3 = (bf16[4,88,384]{2,1,0:T(8,128)(2,1)S(1)}, bf16[4,88,384]{2,1,0:T(8,128)(2,1)S(1)}, u32[]{:S(2)}, u32[]{:S(2)}) collective-permute-start(bf16[4,88,384]{2,1,0:T(8,128)(2,1)S(1)} %get-tuple-element.37), channel_id=1, source_target_pairs={{0,64},{1,961},{64,128},{65,1},{128,192},{129,65},{192,256},{193,1... | collective-permute-start | bytes 811016 | tf_op jit(solution)/shard_map/ppermute | solution.py:279
  74.9 21.0 %collective-permute-start.4 = (bf16[4,88,384]{2,1,0:T(8,128)(2,1)S(1)}, bf16[4,88,384]{2,1,0:T(8,128)(2,1)S(1)}, u32[]{:S(2)}, u32[]{:S(2)}) collective-permute-start(bf16[4,88,384]{2,1,0:T(8,128)(2,1)S(1)} %get-tuple-element.38), channel_id=1, source_target_pairs={{0,960},{1,65},{64,0},{65,129},{128,64},{129,193},{192,128},{193,2... | collective-permute-start | bytes 811016 | tf_op jit(solution)/shard_map/ppermute | solution.py:279
  96.0 19.5 %collective-permute-start.5 = (bf16[88,384]{1,0:T(8,128)(2,1)S(1)}, bf16[88,384]{1,0:T(8,128)(2,1)S(1)}, u32[]{:S(2)}, u32[]{:S(2)}) collective-permute-start(bf16[88,384]{1,0:T(8,128)(2,1)S(1)} %get-tuple-element.40), channel_id=1, source_target_pairs={{0,128},{1,897},{64,192},{65,961},{128,256},{129,1},{192,320},{193... | collective-permute-start | bytes 202760 | tf_op jit(solution)/shard_map/ppermute | solution.py:279
  97.9 17.6 %collective-permute-start.6 = (bf16[88,384]{1,0:T(8,128)(2,1)S(1)}, bf16[88,384]{1,0:T(8,128)(2,1)S(1)}, u32[]{:S(2)}, u32[]{:S(2)}) collective-permute-start(bf16[88,384]{1,0:T(8,128)(2,1)S(1)} %get-tuple-element.41), channel_id=1, source_target_pairs={{0,384},{1,641},{64,448},{65,705},{128,512},{129,769},{192,576},{1... | collective-permute-start | bytes 202760 | tf_op jit(solution)/shard_map/ppermute | solution.py:279
  105.7 12.6 %collective-permute-start.7 = (bf16[88,384]{1,0:T(8,128)(2,1)S(1)}, bf16[88,384]{1,0:T(8,128)(2,1)S(1)}, u32[]{:S(2)}, u32[]{:S(2)}) collective-permute-start(bf16[88,384]{1,0:T(8,128)(2,1)S(1)} %get-tuple-element.42), channel_id=1, source_target_pairs={{0,640},{1,385},{64,704},{65,449},{128,768},{129,513},{192,832},{1... | collective-permute-start | bytes 202760 | tf_op jit(solution)/shard_map/ppermute | solution.py:279
  110.7 8.4 %collective-permute-start.8 = (bf16[88,384]{1,0:T(8,128)(2,1)S(1)}, bf16[88,384]{1,0:T(8,128)(2,1)S(1)}, u32[]{:S(2)}, u32[]{:S(2)}) collective-permute-start(bf16[88,384]{1,0:T(8,128)(2,1)S(1)} %get-tuple-element.43), channel_id=1, source_target_pairs={{0,896},{1,129},{64,960},{65,193},{128,0},{129,257},{192,64},{193,... | collective-permute-start | bytes 202760 | tf_op jit(solution)/shard_map/ppermute | solution.py:279

commit v2 on v1

--- a/solution.py
+++ b/solution.py
@@ -9,7 +9,6 @@
 from jax.sharding import PartitionSpec as P
 
 
-FS_TP = ("fs", "tp_0", "tp_1")
 EPS = 1e-06
 BF = jnp.bfloat16
 F32 = jnp.float32
@@ -83,7 +82,7 @@
     grad_s,
 ):
     n_rep, n_fs, n_x, n_core, tokens, _, padded, width, block = sizes
-    core = lax.axis_index("tp_1")
+    core = lax.rem(lax.axis_index("node"), 2)
     z = lax.axis_index("rep")
     tall = grad_s.shape[1]
     total = square_ref[...] + square_sum(other_ref, tokens)
@@ -91,19 +90,21 @@
     inv = lax.rsqrt(mean + EPS)
     inv_ref[...] = jnp.broadcast_to(inv, (8, tokens))
 
-    def normalise(s, carry):
-        x = n_x - 1 - s // n_fs
-        y = n_fs - 1 - s % n_fs
+    def normalise(first, carry):
         for ref, which in ((own_ref, core), (other_ref, 1 - core)):
-            at = pl.multiple_of(((y * n_x + x) * n_core + which) * block, block)
-            v = ref[s, :, 0:tokens].astype(F32) * inv
-            g = gain_s[pl.ds(at, block), :]
-            v = v * jnp.concatenate([g] * (tokens // LANES), axis=1)
-            normed_s[pl.ds(at, block), :] = v.astype(BF)
-            cot_s[pl.ds(at, block), :] = ref[s, :, tokens : 2 * tokens]
+            for second in range(4):
+                y = 2 * (n_fs // 2 - 1 - first // 2) + lax.rem(1 - second // 2 + which, 2)
+                x = 2 * (n_x // 2 - 1 - lax.rem(first, 2)) + lax.rem(1 - second % 2 + which, 2)
+                at = pl.multiple_of(((y * n_x + x) * n_core + which) * block, block)
+                s = second * 8 + first
+                v = ref[s, :, 0:tokens].astype(F32) * inv
+                g = gain_s[pl.ds(at, block), :]
+                v = v * jnp.concatenate([g] * (tokens // LANES), axis=1)
+                normed_s[pl.ds(at, block), :] = v.astype(BF)
+                cot_s[pl.ds(at, block), :] = ref[s, :, tokens : 2 * tokens]
         return carry
 
-    lax.fori_loop(0, n_fs * n_x, normalise, 0)
+    lax.fori_loop(0, 8, normalise, 0)
 
     both = jnp.dot(pair_s[...], normed_s[...], preferred_element_type=F32)
     d_hidden = 0.5 * jnp.dot(down_s[...], cot_s[...], preferred_element_type=F32)
@@ -210,7 +211,7 @@
     chunk_ref,
     column_s,
 ):
-    n_x, n_core, width, hidden, block = sizes
+    _, _, width, hidden, block = sizes
     sources, rows, _ = part_ref.shape
     tokens = tok_ref.shape[1]
     groups = tokens // LANES
@@ -223,7 +224,7 @@
     at = groups * block
     row = [total[at + k : at + k + 1, :] + total[at + groups + k : at + groups + k + 1, :] for k in range(groups)]
     row = jnp.concatenate(row, axis=1) / width
-    me = (lax.axis_index("fs") * n_x + lax.axis_index("tp_0")) * n_core + lax.axis_index("tp_1")
+    me = lax.axis_index("node")
     per = LANES // block
     mine = gain_ref[pl.ds(lax.div(me, per), 1), :]
     column_s[...] = jnp.broadcast_to(mine, (LANES, LANES)).T
@@ -263,25 +264,50 @@
     gain_ref[...] = gain[:, 0 : gain_ref.shape[1]]
 
 
-def spread(block, axis):
-    n = lax.axis_size(axis)
-    copies = jnp.broadcast_to(block[None], (n,) + block.shape)
-    backwards = [list(range(n - 1, -1, -1))]
-    return lax.all_to_all(copies, axis, 0, 0, tiled=True, axis_index_groups=backwards)
+def spread(block, groups):
+    copies = jnp.broadcast_to(block[None], (len(groups[0]),) + block.shape)
+    return lax.all_to_all(copies, "node", 0, 0, tiled=True, axis_index_groups=groups)
+
+
+def gather_groups(n_fs, n_x):
+    def node(y, x, core):
+        return (y % n_fs * n_x + x % n_x) * 2 + core
+
+    cores, halves = range(2), range(2)
+    wide = [
+        [node(y, x, core) for y in range(n_fs - 2 + p, -1, -2) for x in range(n_x - 2 + q, -1, -2)]
+        for core in cores
+        for p in halves
+        for q in halves
+    ]
+    near = [
+        [node(2 * j + core + a, 2 * i + core + b, core) for a in (1, 0) for b in (1, 0)]
+        for core in cores
+        for j in range(n_fs // 2)
+        for i in range(n_x // 2)
+    ]
+    return wide, near
+
+
+def swapped(v):
+    n = lax.axis_size("node")
+    return lax.ppermute(v, "node", [(k, k ^ 1) for k in range(n)])
 
 
 def shifted(v, by):
-    n = lax.axis_size("rep")
+    n, m = lax.axis_size("rep"), lax.axis_size("node")
     pairs = []
     for z in range(n):
-        pairs.append((z * 2, (z + by) % n * 2))
-        pairs.append((z * 2 + 1, (z - by) % n * 2 + 1))
-    return lax.ppermute(v, ("rep", "tp_1"), pairs)
+        for k in range(m):
+            to = (z - by if k % 2 else z + by) % n
+            pairs.append((z * m + k, to * m + k))
+    return lax.ppermute(v, ("rep", "node"), pairs)
 
 
 def body(tokens, cotangent, gain, w_gate, w_up, w_down):
     n_rep = lax.axis_size("rep")
-    n_fs, n_x, n_core = (lax.axis_size(a) for a in FS_TP)
+    n_fs, n_x, n_core = 8, 4, 2
+    wide, near = gather_groups(n_fs, n_x)
     peers = n_fs * n_x
     rows, block = tokens.shape
     width = gain.shape[0]
@@ -291,10 +317,10 @@
     n_blocks = width // LANES
     tok_t, cot_t = tokens.T, cotangent.T
     both = jnp.concatenate([tok_t, cot_t], axis=1)
-    column = spread(both, "fs")
-    plane = spread(column.reshape(n_fs * block, 2 * rows), "tp_0")
+    patch = spread(both, wide)
+    plane = spread(patch.reshape(8 * block, 2 * rows), near)
     plane = plane.reshape(peers, block, 2 * rows)
-    other = lax.ppermute(plane, "tp_1", [(0, 1), (1, 0)])
+    other = swapped(plane)
     gain_rows = gain.reshape(n_blocks, LANES)
 
     def shape(*dims, dtype=BF):
@@ -344,7 +370,7 @@
         name="main",
     )(plane, other, pair, down, columns, square)
 
-    got = lax.ppermute(send, "tp_1", [(0, 1), (1, 0)])
+    got = swapped(send)
     far = shifted(far, 2)
     near = shifted(near, 1)
     back = shifted(back, -1)
@@ -361,7 +387,8 @@
         cost_estimate=pl.CostEstimate(flops=10**6, bytes_accessed=3 * 10**6, transcendentals=0),
         name="core",
     )(keep, got, row)
-    parts = lax.all_to_all(ready, FS_TP[:2], 0, 0, tiled=True)
+    across = [[k * 2 + core for k in range(peers)] for core in range(2)]
+    parts = lax.all_to_all(ready, "node", 0, 0, tiled=True, axis_index_groups=across)
     sums = pl.pallas_call(
         stop_kernel,
         out_shape=[shape(tall, 3 * LANES)] * 4,
@@ -401,14 +428,14 @@
 
 def solution(mesh):
     torus = Mesh(
-        mesh.devices.reshape(mesh.shape["rep"], mesh.shape["fs"], 4, 2),
-        ("rep", "fs", "tp_0", "tp_1"),
+        mesh.devices.reshape(mesh.shape["rep"], 64),
+        ("rep", "node"),
     )
-    placed = (P("rep", FS_TP), P("rep", FS_TP), P(), P(FS_TP, None), P(FS_TP, None), P(FS_TP, None))
+    placed = (P("rep", "node"), P("rep", "node"), P(), P("node", None), P("node", None), P("node", None))
     return jax.shard_map(
         body,
         mesh=torus,
         in_specs=placed,
-        out_specs=(P("rep", FS_TP), P(FS_TP), P(FS_TP, None), P(FS_TP, None), P(FS_TP, None)),
+        out_specs=(P("rep", "node"), P("node"), P("node", None), P("node", None), P("node", None)),
         check_vma=False,
     )

time: 156 us -> 152 us (0.974)
  starting transfers between devices: 54.1 us -> 49.6 us
    ppermute x9, starting transfers between devices: 45.5 us -> 40.5 us  [the longest x7 36.6 us: shifted(): return lax.ppermute(v, ('rep', 'node'), pairs)]
where the time goes in v2:
time: 152 us
  blocking collectives  75.3 us (50%)
  starting transfers between devices  49.6 us (33%)
  waiting for transfers between devices  17.7 us (12%)
  Pallas kernels  7.24 us (5%)
    all_to_all x2, blocking collectives, spread(): lax.all_to_all(copies, 'node', 0, 0, tiled=True, axis_index_groups=groups)  41 us
    ppermute x7, starting transfers between devices, shifted(): return lax.ppermute(v, ('rep', 'node'), pairs)  36.6 us
    all_gather x1, blocking collectives, body(): everything = lax.all_gather(chunk, 'rep', axis=0, tiled=False)  34.3 us
    ppermute x7, waiting for transfers between devices, shifted(): return lax.ppermute(v, ('rep', 'node'), pairs)  12.8 us
    all_to_all x1, starting transfers between devices, body(): lax.all_to_all(ready, 'node', 0, 0, tiled=True, axis_index_groups=across)  9.09 us
    ppermute x2, waiting for transfers between devices, swapped(): return lax.ppermute(v, 'node', [(k, k ^ 1) for k in range(n)])  4.96 us
    ppermute x2, starting transfers between devices, swapped(): return lax.ppermute(v, 'node', [(k, k ^ 1) for k in range(n)])  3.96 us
    pallas_call x1, Pallas kernels, body(): pl.pallas_call(functools.partial(main_kernel, sizes), out_shape=[shape(pe...  3.77 us
  transfers between devices with their start and end apart: 10, of which 6 were waited for; matrix products, arithmetic and copies ran while one was open for 0% of the time, Pallas kernels for 0%

profile of v2, /device:TPU:6, one launch (start us, length us, event | category | flops | bytes accessed | tf_op | source)
XLA Modules:
  0.0 151.7 jit_solution(15596728785478681729)
XLA Ops:
  0.6 0.8 pad_maximum_fusion
  1.4 21.9 %all_to_all.15 = bf16[8,32,768]{2,1,0:T(8,128)(2,1)S(1)} all-to-all(bf16[8,32,768]{2,1,0:T(8,128)(2,1)S(1)} %broadcast_in_dim.6), channel_id=1, replica_groups={{52,48,36,32,20,16,4,0},{54,50,38,34,22,18,6,2},{60,56,44,40,28,24,12,8..., dimensions={0} | all-to-all | bytes 786432 | tf_op jit(solution)/shard_map/all_to_all | solution.py:269
  23.3 0.1 broadcast_in_dim.15
  23.4 0.0 copy-start
  23.4 0.0 copy-start.1
  23.4 0.0 copy-start.2
  23.4 0.0 copy-start.5
  23.4 19.1 %all_to_all.16 = bf16[4,256,768]{2,1,0:T(8,128)(2,1)S(1)} all-to-all(bf16[4,256,768]{2,1,0:T(8,128)(2,1)S(1)} %broadcast_in_dim.15), channel_id=1, replica_groups={{10,8,2,0},{14,12,6,4},{26,24,18,16},{30,28,22,20},{42,40,34,32},{46,44..., dimensions={0} | all-to-all | bytes 3145728 | tf_op jit(solution)/shard_map/all_to_all | solution.py:269
  42.6 1.9 %collective-permute-start = (bf16[32,32,768]{2,1,0:T(8,128)(2,1)S(1)}, bf16[32,32,768]{2,1,0:T(8,128)(2,1)S(1)}, u32[]{:S(2)}, u32[]{:S(2)}) collective-permute-start(bf16[32,32,768]{2,1,0:T(8,128)(2,1)S(1)} %bitcast.8), channel_id=1, source_target_pairs={{0,1},{1,0},{2,3},{3,2},{4,5},{5,4},{6,7},{7,6},{8,9},{9,8},{10,11... | collective-permute-start | bytes 4718600 | tf_op jit(solution)/shard_map/ppermute | solution.py:294
  44.5 0.0 copy-done
  44.5 0.0 copy-done.1
  44.5 0.0 copy-done.2
  44.5 0.0 copy-done.5
  44.5 0.5 ready.1
  45.1 2.8 %collective-permute-done.other_ref = bf16[32,32,768]{2,1,0:T(8,128)(2,1)S(1)} collective-permute-done((bf16[32,32,768]{2,1,0:T(8,128)(2,1)S(1)}, bf16[32,32,768]{2,1,0:T(8,128)(2,1)S(1)}, u32[]{:S(2)}, u32[]{:S(2)}) %collective-permute-start) | collective-permute-done | bytes 1572896 | tf_op jit(solution)/shard_map/ppermute | solution.py:294
  47.9 3.8 %main.1 = (bf16[32,32,384]{2,1,0:T(8,128)(2,1)S(1)}, bf16[33,32,384]{2,1,0:T(8,128)(2,1)S(1)}, f32[8,384]{1,0:T(8,128)S(1)}, f32[8,384]{1,0:T(8,128)S(1)}, bf16[...) custom-call(bf16[32,32,768]{2,1,0:T(8,128)(2,1)S(1)} %bitcast.10, ...), custom_call_target="tpu_custom_call" | custom-call | flops 1100000000 | bytes 10000000 | tf_op jit(solution)/shard_map/main/pallas_call | solution.py:346
  51.6 2.1 %collective-permute-start.1 = (bf16[33,32,384]{2,1,0:T(8,128)(2,1)S(1)}, bf16[33,32,384]{2,1,0:T(8,128)(2,1)S(1)}, u32[]{:S(2)}, u32[]{:S(2)}) collective-permute-start(bf16[33,32,384]{2,1,0:T(8,128)(2,1)S(1)} %get-tuple-element.33), channel_id=1, source_target_pairs={{0,1},{1,0},{2,3},{3,2},{4,5},{5,4},{6,7},{7,6},{8,9},{9,8},{10,11... | collective-permute-start | bytes 2433032 | tf_op jit(solution)/shard_map/ppermute | solution.py:294
  53.7 2.2 %collective-permute-done.1.got_ref = bf16[33,32,384]{2,1,0:T(8,128)(2,1)S(1)} collective-permute-done((bf16[33,32,384]{2,1,0:T(8,128)(2,1)S(1)}, bf16[33,32,384]{2,1,0:T(8,128)(2,1)S(1)}, u32[]{:S(2)}, u32[]{:S(2)}) %collective-permute-start.1) | collective-permute-done | bytes 811040 | tf_op jit(solution)/shard_map/ppermute | solution.py:294
  55.8 1.0 core.1
  56.9 0.0 copy-start.3
  56.9 0.0 copy-start.4
  56.9 9.1 %all-to-all-start.2 = ((bf16[32,104,128]{2,1,0:T(8,128)(2,1)}), bf16[32,104,128]{2,1,0:T(8,128)(2,1)S(1)}, u32[]{:S(2)}, u32[]{:S(2)}) async-start(bf16[32,104,128]{2,1,0:T(8,128)(2,1)} %core.1), calls=%async_computation.2 | async-start | bytes 1703936 | tf_op jit(solution)/shard_map/all_to_all | solution.py:391
  66.0 1.9 %collective-permute-start.2 = (bf16[4,88,384]{2,1,0:T(8,128)(2,1)S(1)}, bf16[4,88,384]{2,1,0:T(8,128)(2,1)S(1)}, u32[]{:S(2)}, u32[]{:S(2)}) collective-permute-start(bf16[4,88,384]{2,1,0:T(8,128)(2,1)S(1)} %get-tuple-element.36), channel_id=1, source_target_pairs={{0,128},{1,897},{2,130},{3,899},{4,132},{5,901},{6,134},{7,903},{8... | collective-permute-start | bytes 811016 | tf_op jit(solution)/shard_map/ppermute | solution.py:304
  67.9 3.4 %collective-permute-start.3 = (bf16[4,88,384]{2,1,0:T(8,128)(2,1)S(1)}, bf16[4,88,384]{2,1,0:T(8,128)(2,1)S(1)}, u32[]{:S(2)}, u32[]{:S(2)}) collective-permute-start(bf16[4,88,384]{2,1,0:T(8,128)(2,1)S(1)} %get-tuple-element.37), channel_id=1, source_target_pairs={{0,64},{1,961},{2,66},{3,963},{4,68},{5,965},{6,70},{7,967},{8,72}... | collective-permute-start | bytes 811016 | tf_op jit(solution)/shard_map/ppermute | solution.py:304
  71.4 11.7 %collective-permute-start.4 = (bf16[4,88,384]{2,1,0:T(8,128)(2,1)S(1)}, bf16[4,88,384]{2,1,0:T(8,128)(2,1)S(1)}, u32[]{:S(2)}, u32[]{:S(2)}) collective-permute-start(bf16[4,88,384]{2,1,0:T(8,128)(2,1)S(1)} %get-tuple-element.38), channel_id=1, source_target_pairs={{0,960},{1,65},{2,962},{3,67},{4,964},{5,69},{6,966},{7,71},{8,968... | collective-permute-start | bytes 811016 | tf_op jit(solution)/shard_map/ppermute | solution.py:304
  83.1 0.7 collective-permute-done.2.far_ref
  83.7 8.6 %collective-permute-done.3.near_ref = bf16[4,88,384]{2,1,0:T(8,128)(2,1)S(1)} collective-permute-done((bf16[4,88,384]{2,1,0:T(8,128)(2,1)S(1)}, bf16[4,88,384]{2,1,0:T(8,128)(2,1)S(1)}, u32[]{:S(2)}, u32[]{:S(2)}) %collective-permute-start.3) | collective-permute-done | bytes 270368 | tf_op jit(solution)/shard_map/ppermute | solution.py:304
  92.3 0.0 collective-permute-done.4.back_ref
  92.3 0.1 stop.1
  92.5 1.9 %collective-permute-start.5 = (bf16[88,384]{1,0:T(8,128)(2,1)S(1)}, bf16[88,384]{1,0:T(8,128)(2,1)S(1)}, u32[]{:S(2)}, u32[]{:S(2)}) collective-permute-start(bf16[88,384]{1,0:T(8,128)(2,1)S(1)} %get-tuple-element.40), channel_id=1, source_target_pairs={{0,128},{1,897},{2,130},{3,899},{4,132},{5,901},{6,134},{7,903},{8... | collective-permute-start | bytes 202760 | tf_op jit(solution)/shard_map/ppermute | solution.py:304
  94.4 7.7 %collective-permute-start.6 = (bf16[88,384]{1,0:T(8,128)(2,1)S(1)}, bf16[88,384]{1,0:T(8,128)(2,1)S(1)}, u32[]{:S(2)}, u32[]{:S(2)}) collective-permute-start(bf16[88,384]{1,0:T(8,128)(2,1)S(1)} %get-tuple-element.41), channel_id=1, source_target_pairs={{0,384},{1,641},{2,386},{3,643},{4,388},{5,645},{6,390},{7,647},{8... | collective-permute-start | bytes 202760 | tf_op jit(solution)/shard_map/ppermute | solution.py:304
  102.1 5.0 %collective-permute-start.7 = (bf16[88,384]{1,0:T(8,128)(2,1)S(1)}, bf16[88,384]{1,0:T(8,128)(2,1)S(1)}, u32[]{:S(2)}, u32[]{:S(2)}) collective-permute-start(bf16[88,384]{1,0:T(8,128)(2,1)S(1)} %get-tuple-element.42), channel_id=1, source_target_pairs={{0,640},{1,385},{2,642},{3,387},{4,644},{5,389},{6,646},{7,391},{8... | collective-permute-start | bytes 202760 | tf_op jit(solution)/shard_map/ppermute | solution.py:304
  107.2 4.8 %collective-permute-start.8 = (bf16[88,384]{1,0:T(8,128)(2,1)S(1)}, bf16[88,384]{1,0:T(8,128)(2,1)S(1)}, u32[]{:S(2)}, u32[]{:S(2)}) collective-permute-start(bf16[88,384]{1,0:T(8,128)(2,1)S(1)} %get-tuple-element.43), channel_id=1, source_target_pairs={{0,896},{1,129},{2,898},{3,131},{4,900},{5,133},{6,902},{7,135},{8... | collective-permute-start | bytes 202760 | tf_op jit(solution)/shard_map/ppermute | solution.py:304
  112.0 0.0 collective-permute-done.5.a_ref
  112.0 0.0 collective-permute-done.6.b_ref
  112.0 2.7 %collective-permute-done.7.c_ref = bf16[88,384]{1,0:T(8,128)(2,1)S(1)} collective-permute-done((bf16[88,384]{1,0:T(8,128)(2,1)S(1)}, bf16[88,384]{1,0:T(8,128)(2,1)S(1)}, u32[]{:S(2)}, u32[]{:S(2)}) %collective-permute-start.7) | collective-permute-done | bytes 67616 | tf_op jit(solution)/shard_map/ppermute | solution.py:304
  114.8 0.8 collective-permute-done.8.d_ref
  115.6 0.0 all-to-all-done.2.part_ref
  115.6 0.0 copy-done.3
  115.6 0.0 copy-done.4
  115.6 0.3 owner.1
  115.9 34.3 %all-gather.1.all_ref = bf16[16,85,384]{2,1,0:T(8,128)(2,1)S(1)} all-gather(bf16[1,85,384]{2,1,0:T(8,128)(2,1)S(1)} %bitcast.15), channel_id=2, replica_groups=mesh['rep'=16,'fs'=8,'tp'=8] {'rep'}, dimensions={0}, use_global_device_ids=true | all-gather | bytes 1109760 | tf_op jit(solution)/shard_map/all_gather | solution.py:416
  150.2 1.5 out.1
  (1 shorter events, 0.0 us)
Async XLA Ops:
  23.4 21.1 %copy-start = (bf16[84,2048]{1,0:T(8,128)(2,1)S(1)}, bf16[84,2048]{1,0:T(8,128)(2,1)}, u32[]{:S(2)}) copy-start(bf16[84,2048]{1,0:T(8,128)(2,1)} %gate_w_ref.1) | copy-start | bytes 1032196
  23.4 21.1 %copy-start.1 = (bf16[84,2048]{1,0:T(8,128)(2,1)S(1)}, bf16[84,2048]{1,0:T(8,128)(2,1)}, u32[]{:S(2)}) copy-start(bf16[84,2048]{1,0:T(8,128)(2,1)} %up_w_ref.1) | copy-start | bytes 1032196
  23.4 21.1 %copy-start.2 = (bf16[84,2048]{1,0:T(8,128)(2,1)S(1)}, bf16[84,2048]{1,0:T(8,128)(2,1)}, u32[]{:S(2)}) copy-start(bf16[84,2048]{1,0:T(8,128)(2,1)} %down_w_ref.1) | copy-start | bytes 1032196
  23.4 21.1 %copy-start.5 = (f32[2048]{0:T(1024)S(1)}, f32[2048]{0:T(1024)}, u32[]{:S(2)}) copy-start(f32[2048]{0:T(1024)} %param.8) | copy-start | bytes 24580
  42.6 5.3 %collective-permute-start = (bf16[32,32,768]{2,1,0:T(8,128)(2,1)S(1)}, bf16[32,32,768]{2,1,0:T(8,128)(2,1)S(1)}, u32[]{:S(2)}, u32[]{:S(2)}) collective-permute-start(bf16[32,32,768]{2,1,0:T(8,128)(2,1)S(1)} %bitcast.8), channel_id=1, source_target_pairs={{0,1},{1,0},{2,3},{3,2},{4,5},{5,4},{6,7},{7,6},{8,9},{9,8},{10,11... | collective-permute-start | bytes 4718600 | tf_op jit(solution)/shard_map/ppermute | solution.py:294
  51.6 4.2 %collective-permute-start.1 = (bf16[33,32,384]{2,1,0:T(8,128)(2,1)S(1)}, bf16[33,32,384]{2,1,0:T(8,128)(2,1)S(1)}, u32[]{:S(2)}, u32[]{:S(2)}) collective-permute-start(bf16[33,32,384]{2,1,0:T(8,128)(2,1)S(1)} %get-tuple-element.33), channel_id=1, source_target_pairs={{0,1},{1,0},{2,3},{3,2},{4,5},{5,4},{6,7},{7,6},{8,9},{9,8},{10,11... | collective-permute-start | bytes 2433032 | tf_op jit(solution)/shard_map/ppermute | solution.py:294
  56.9 58.7 %copy-start.3 = (bf16[384,32]{0,1:T(8,128)(2,1)S(1)}, bf16[384,32]{0,1:T(8,128)(2,1)}, u32[]{:S(2)}) copy-start(bf16[384,32]{0,1:T(8,128)(2,1)} %param.7) | copy-start | bytes 73732
  56.9 58.7 %copy-start.4 = (bf16[384,32]{0,1:T(8,128)(2,1)S(1)}, bf16[384,32]{0,1:T(8,128)(2,1)}, u32[]{:S(2)}) copy-start(bf16[384,32]{0,1:T(8,128)(2,1)} %param.6) | copy-start | bytes 73732
  56.9 58.7 %all-to-all-start.2 = ((bf16[32,104,128]{2,1,0:T(8,128)(2,1)}), bf16[32,104,128]{2,1,0:T(8,128)(2,1)S(1)}, u32[]{:S(2)}, u32[]{:S(2)}) async-start(bf16[32,104,128]{2,1,0:T(8,128)(2,1)} %core.1), calls=%async_computation.2 | async-start | bytes 1703936 | tf_op jit(solution)/shard_map/all_to_all | solution.py:391
  66.0 17.7 %collective-permute-start.2 = (bf16[4,88,384]{2,1,0:T(8,128)(2,1)S(1)}, bf16[4,88,384]{2,1,0:T(8,128)(2,1)S(1)}, u32[]{:S(2)}, u32[]{:S(2)}) collective-permute-start(bf16[4,88,384]{2,1,0:T(8,128)(2,1)S(1)} %get-tuple-element.36), channel_id=1, source_target_pairs={{0,128},{1,897},{2,130},{3,899},{4,132},{5,901},{6,134},{7,903},{8... | collective-permute-start | bytes 811016 | tf_op jit(solution)/shard_map/ppermute | solution.py:304
  67.9 24.4 %collective-permute-start.3 = (bf16[4,88,384]{2,1,0:T(8,128)(2,1)S(1)}, bf16[4,88,384]{2,1,0:T(8,128)(2,1)S(1)}, u32[]{:S(2)}, u32[]{:S(2)}) collective-permute-start(bf16[4,88,384]{2,1,0:T(8,128)(2,1)S(1)} %get-tuple-element.37), channel_id=1, source_target_pairs={{0,64},{1,961},{2,66},{3,963},{4,68},{5,965},{6,70},{7,967},{8,72}... | collective-permute-start | bytes 811016 | tf_op jit(solution)/shard_map/ppermute | solution.py:304
  71.4 21.0 %collective-permute-start.4 = (bf16[4,88,384]{2,1,0:T(8,128)(2,1)S(1)}, bf16[4,88,384]{2,1,0:T(8,128)(2,1)S(1)}, u32[]{:S(2)}, u32[]{:S(2)}) collective-permute-start(bf16[4,88,384]{2,1,0:T(8,128)(2,1)S(1)} %get-tuple-element.38), channel_id=1, source_target_pairs={{0,960},{1,65},{2,962},{3,67},{4,964},{5,69},{6,966},{7,71},{8,968... | collective-permute-start | bytes 811016 | tf_op jit(solution)/shard_map/ppermute | solution.py:304
  92.5 19.5 %collective-permute-start.5 = (bf16[88,384]{1,0:T(8,128)(2,1)S(1)}, bf16[88,384]{1,0:T(8,128)(2,1)S(1)}, u32[]{:S(2)}, u32[]{:S(2)}) collective-permute-start(bf16[88,384]{1,0:T(8,128)(2,1)S(1)} %get-tuple-element.40), channel_id=1, source_target_pairs={{0,128},{1,897},{2,130},{3,899},{4,132},{5,901},{6,134},{7,903},{8... | collective-permute-start | bytes 202760 | tf_op jit(solution)/shard_map/ppermute | solution.py:304
  94.4 17.6 %collective-permute-start.6 = (bf16[88,384]{1,0:T(8,128)(2,1)S(1)}, bf16[88,384]{1,0:T(8,128)(2,1)S(1)}, u32[]{:S(2)}, u32[]{:S(2)}) collective-permute-start(bf16[88,384]{1,0:T(8,128)(2,1)S(1)} %get-tuple-element.41), channel_id=1, source_target_pairs={{0,384},{1,641},{2,386},{3,643},{4,388},{5,645},{6,390},{7,647},{8... | collective-permute-start | bytes 202760 | tf_op jit(solution)/shard_map/ppermute | solution.py:304
  102.1 12.6 %collective-permute-start.7 = (bf16[88,384]{1,0:T(8,128)(2,1)S(1)}, bf16[88,384]{1,0:T(8,128)(2,1)S(1)}, u32[]{:S(2)}, u32[]{:S(2)}) collective-permute-start(bf16[88,384]{1,0:T(8,128)(2,1)S(1)} %get-tuple-element.42), channel_id=1, source_target_pairs={{0,640},{1,385},{2,642},{3,387},{4,644},{5,389},{6,646},{7,391},{8... | collective-permute-start | bytes 202760 | tf_op jit(solution)/shard_map/ppermute | solution.py:304
  107.2 8.4 %collective-permute-start.8 = (bf16[88,384]{1,0:T(8,128)(2,1)S(1)}, bf16[88,384]{1,0:T(8,128)(2,1)S(1)}, u32[]{:S(2)}, u32[]{:S(2)}) collective-permute-start(bf16[88,384]{1,0:T(8,128)(2,1)S(1)} %get-tuple-element.43), channel_id=1, source_target_pairs={{0,896},{1,129},{2,898},{3,131},{4,900},{5,133},{6,902},{7,135},{8... | collective-permute-start | bytes 202760 | tf_op jit(solution)/shard_map/ppermute | solution.py:304

commit v3 on v2

--- a/solution.py
+++ b/solution.py
@@ -13,6 +13,7 @@
 BF = jnp.bfloat16
 F32 = jnp.float32
 LANES = 128
+FIRST = 12
 VMEM = pl.BlockSpec(memory_space=pltpu.VMEM)
 ANY = pl.BlockSpec(memory_space=pl.ANY)
 
@@ -93,7 +94,7 @@
     def normalise(first, carry):
         for ref, which in ((own_ref, core), (other_ref, 1 - core)):
             for second in range(4):
-                y = 2 * (n_fs // 2 - 1 - first // 2) + lax.rem(1 - second // 2 + which, 2)
+                y = 2 * lax.rem(n_fs // 2 - 1 - first // 2 + 3, n_fs // 2) + lax.rem(second // 2 + which, 2)
                 x = 2 * (n_x // 2 - 1 - lax.rem(first, 2)) + lax.rem(1 - second % 2 + which, 2)
                 at = pl.multiple_of(((y * n_x + x) * n_core + which) * block, block)
                 s = second * 8 + first
@@ -157,7 +158,7 @@
             grad_s[at, :, 2 * LANES : 3 * LANES] = one[0:tall, lanes].astype(BF)
 
     for i in range(4):
-        for ref, base in ((far_ref, 4), (near_ref, 3), (back_ref, 1), (stay_ref, 2)):
+        for ref, base in ((far_ref, 2), (near_ref, 1), (back_ref, -1), (stay_ref, 0)):
             ref[i] = grad_s[lax.rem(z + side * (base + 4 * i) + 2 * n_rep, n_rep)]
 
 
@@ -172,11 +173,12 @@
     tail = [v[:, k * LANES : (k + 1) * LANES] for v in (high, low_part) for k in range(groups)]
     tail = jnp.concatenate(tail + [jnp.zeros((8 - 2 * groups, LANES), BF)], axis=0)
 
-    def add(s, carry):
-        v = (keep_ref[s].astype(F32) + got_ref[s].astype(F32)).astype(BF)
+    def add(at, carry):
+        s = lax.rem(at + FIRST, slabs)
+        v = keep_ref[s] + got_ref[s]
         for k in range(groups):
-            slab_s[s, k * block : (k + 1) * block, :] = v[:, k * LANES : (k + 1) * LANES]
-        slab_s[s, groups * block : groups * block + 8, :] = tail
+            slab_s[at, k * block : (k + 1) * block, :] = v[:, k * LANES : (k + 1) * LANES]
+        slab_s[at, groups * block : groups * block + 8, :] = tail
         return carry
 
     copies = []
@@ -193,7 +195,7 @@
     for i, out_ref in enumerate(out_refs):
         v = stay_ref[i].astype(F32) + far_ref[i].astype(F32)
         v = v + near_ref[i].astype(F32) + back_ref[i].astype(F32)
-        out_ref[...] = v.astype(BF)
+        out_ref[...] = v.astype(out_ref.dtype)
 
 
 def owner_kernel(
@@ -275,13 +277,13 @@
 
     cores, halves = range(2), range(2)
     wide = [
-        [node(y, x, core) for y in range(n_fs - 2 + p, -1, -2) for x in range(n_x - 2 + q, -1, -2)]
+        [node(y, x, core) for y in [(k + 6) % n_fs + p for k in range(n_fs - 2, -1, -2)] for x in range(n_x - 2 + q, -1, -2)]
         for core in cores
         for p in halves
         for q in halves
     ]
     near = [
-        [node(2 * j + core + a, 2 * i + core + b, core) for a in (1, 0) for b in (1, 0)]
+        [node(2 * j + core + a, 2 * i + core + b, core) for a in (0, 1) for b in (1, 0)]
         for core in cores
         for j in range(n_fs // 2)
         for i in range(n_x // 2)
@@ -387,19 +389,19 @@
         cost_estimate=pl.CostEstimate(flops=10**6, bytes_accessed=3 * 10**6, transcendentals=0),
         name="core",
     )(keep, got, row)
-    across = [[k * 2 + core for k in range(peers)] for core in range(2)]
+    across = [[(k + FIRST) % peers * 2 + core for k in range(peers)] for core in range(2)]
     parts = lax.all_to_all(ready, "node", 0, 0, tiled=True, axis_index_groups=across)
     sums = pl.pallas_call(
         stop_kernel,
-        out_shape=[shape(tall, 3 * LANES)] * 4,
+        out_shape=[shape(tall, 3 * LANES, dtype=F32)] + [shape(tall, 3 * LANES)] * 3,
         in_specs=[VMEM] * 4,
         out_specs=[VMEM] * 4,
         compiler_params=pltpu.CompilerParams(vmem_limit_bytes=8 * 2**20),
         cost_estimate=pl.CostEstimate(flops=10**6, bytes_accessed=2 * 10**6, transcendentals=0),
         name="stop",
     )(far, near, back, stay)
-    moved = []
-    for k, by in enumerate((2, 6, -6, -2)):
+    moved = [sums[0]]
+    for k, by in ((1, 4), (2, 8), (3, -4)):
         moved.append(shifted(sums[k], by))
     sums = moved
 

time: 152 us -> 153 us (level)
  waiting for transfers between devices: 17.7 us -> 22.5 us
  starting transfers between devices: 49.6 us -> 45.5 us
    ppermute x7 -> x6, waiting for transfers between devices: 12.8 us -> 17.5 us  [shifted(): return lax.ppermute(v, ('rep', 'node'), pairs)]
    ppermute x7 -> x6, starting transfers between devices: 36.6 us -> 32.9 us  [shifted(): return lax.ppermute(v, ('rep', 'node'), pairs)]
    all_gather x1, blocking collectives: 34.3 us -> 32.8 us  [body(): everything = lax.all_gather(chunk, 'rep', axis=0, tiled=False)]
  transfers between devices with their start and end apart: 10 -> 9, of which waited for: 6 -> 6; matrix products, arithmetic and copies ran while one was open for 0% -> 0% of each run, Pallas kernels for 0% -> 0%
where the time goes in v3:
time: 153 us; the launch traced here: 152 us
  blocking collectives  75.1 us (49%)
  starting transfers between devices  45.5 us (30%)
  waiting for transfers between devices  22.5 us (15%)
  Pallas kernels  7.26 us (5%)
    all_to_all x2, blocking collectives, spread(): lax.all_to_all(copies, 'node', 0, 0, tiled=True, axis_index_groups=groups)  42.3 us
    ppermute x6, starting transfers between devices, shifted(): return lax.ppermute(v, ('rep', 'node'), pairs)  32.9 us
    all_gather x1, blocking collectives, body(): everything = lax.all_gather(chunk, 'rep', axis=0, tiled=False)  32.8 us
    ppermute x6, waiting for transfers between devices, shifted(): return lax.ppermute(v, ('rep', 'node'), pairs)  17.5 us
    all_to_all x1, starting transfers between devices, body(): lax.all_to_all(ready, 'node', 0, 0, tiled=True, axis_index_groups=across)  8.7 us
    ppermute x2, waiting for transfers between devices, swapped(): return lax.ppermute(v, 'node', [(k, k ^ 1) for k in range(n)])  4.96 us
    ppermute x2, starting transfers between devices, swapped(): return lax.ppermute(v, 'node', [(k, k ^ 1) for k in range(n)])  3.95 us
    pallas_call x1, Pallas kernels, body(): pl.pallas_call(functools.partial(main_kernel, sizes), out_shape=[shape(pe...  3.8 us
  transfers between devices with their start and end apart: 9, of which 6 were waited for; matrix products, arithmetic and copies ran while one was open for 0% of the time, Pallas kernels for 0%

profile of v3, /device:TPU:6, one launch (start us, length us, event | category | flops | bytes accessed | tf_op | source)
XLA Modules:
  0.0 152.1 jit_solution(9943785134258865099)
XLA Ops:
  0.6 0.8 pad_maximum_fusion
  1.4 19.7 %all_to_all.15 = bf16[8,32,768]{2,1,0:T(8,128)(2,1)S(1)} all-to-all(bf16[8,32,768]{2,1,0:T(8,128)(2,1)S(1)} %broadcast_in_dim.6), channel_id=1, replica_groups={{36,32,20,16,4,0,52,48},{38,34,22,18,6,2,54,50},{44,40,28,24,12,8,60,56..., dimensions={0} | all-to-all | bytes 786432 | tf_op jit(solution)/shard_map/all_to_all | solution.py:271
  21.2 0.1 broadcast_in_dim.15
  21.3 0.0 copy-start
  21.3 0.0 copy-start.1
  21.3 0.0 copy-start.2
  21.3 0.0 copy-start.5
  21.3 22.6 %all_to_all.16 = bf16[4,256,768]{2,1,0:T(8,128)(2,1)S(1)} all-to-all(bf16[4,256,768]{2,1,0:T(8,128)(2,1)S(1)} %broadcast_in_dim.15), channel_id=1, replica_groups={{2,0,10,8},{6,4,14,12},{18,16,26,24},{22,20,30,28},{34,32,42,40},{38,36..., dimensions={0} | all-to-all | bytes 3145728 | tf_op jit(solution)/shard_map/all_to_all | solution.py:271
  43.9 1.9 %collective-permute-start = (bf16[32,32,768]{2,1,0:T(8,128)(2,1)S(1)}, bf16[32,32,768]{2,1,0:T(8,128)(2,1)S(1)}, u32[]{:S(2)}, u32[]{:S(2)}) collective-permute-start(bf16[32,32,768]{2,1,0:T(8,128)(2,1)S(1)} %bitcast.8), channel_id=1, source_target_pairs={{0,1},{1,0},{2,3},{3,2},{4,5},{5,4},{6,7},{7,6},{8,9},{9,8},{10,11... | collective-permute-start | bytes 4718600 | tf_op jit(solution)/shard_map/ppermute | solution.py:296
  45.8 0.0 copy-done
  45.8 0.0 copy-done.1
  45.8 0.0 copy-done.2
  45.8 0.0 copy-done.5
  45.9 0.5 ready.1
  46.4 2.8 %collective-permute-done.other_ref = bf16[32,32,768]{2,1,0:T(8,128)(2,1)S(1)} collective-permute-done((bf16[32,32,768]{2,1,0:T(8,128)(2,1)S(1)}, bf16[32,32,768]{2,1,0:T(8,128)(2,1)S(1)}, u32[]{:S(2)}, u32[]{:S(2)}) %collective-permute-start) | collective-permute-done | bytes 1572896 | tf_op jit(solution)/shard_map/ppermute | solution.py:296
  49.2 3.8 %main.1 = (bf16[32,32,384]{2,1,0:T(8,128)(2,1)S(1)}, bf16[33,32,384]{2,1,0:T(8,128)(2,1)S(1)}, f32[8,384]{1,0:T(8,128)S(1)}, f32[8,384]{1,0:T(8,128)S(1)}, bf16[...) custom-call(bf16[32,32,768]{2,1,0:T(8,128)(2,1)S(1)} %bitcast.10, ...), custom_call_target="tpu_custom_call" | custom-call | flops 1100000000 | bytes 10000000 | tf_op jit(solution)/shard_map/main/pallas_call | solution.py:348
  53.0 2.0 %collective-permute-start.1 = (bf16[33,32,384]{2,1,0:T(8,128)(2,1)S(1)}, bf16[33,32,384]{2,1,0:T(8,128)(2,1)S(1)}, u32[]{:S(2)}, u32[]{:S(2)}) collective-permute-start(bf16[33,32,384]{2,1,0:T(8,128)(2,1)S(1)} %get-tuple-element.33), channel_id=1, source_target_pairs={{0,1},{1,0},{2,3},{3,2},{4,5},{5,4},{6,7},{7,6},{8,9},{9,8},{10,11... | collective-permute-start | bytes 2433032 | tf_op jit(solution)/shard_map/ppermute | solution.py:296
  55.0 2.2 %collective-permute-done.1.got_ref = bf16[33,32,384]{2,1,0:T(8,128)(2,1)S(1)} collective-permute-done((bf16[33,32,384]{2,1,0:T(8,128)(2,1)S(1)}, bf16[33,32,384]{2,1,0:T(8,128)(2,1)S(1)}, u32[]{:S(2)}, u32[]{:S(2)}) %collective-permute-start.1) | collective-permute-done | bytes 811040 | tf_op jit(solution)/shard_map/ppermute | solution.py:296
  57.2 1.0 core.1
  58.2 0.0 copy-start.3
  58.2 0.0 copy-start.4
  58.2 8.7 %all-to-all-start.2 = ((bf16[32,104,128]{2,1,0:T(8,128)(2,1)}), bf16[32,104,128]{2,1,0:T(8,128)(2,1)S(1)}, u32[]{:S(2)}, u32[]{:S(2)}) async-start(bf16[32,104,128]{2,1,0:T(8,128)(2,1)} %core.1), calls=%async_computation.2 | async-start | bytes 1703936 | tf_op jit(solution)/shard_map/all_to_all | solution.py:393
  67.0 1.9 %collective-permute-start.2 = (bf16[4,88,384]{2,1,0:T(8,128)(2,1)S(1)}, bf16[4,88,384]{2,1,0:T(8,128)(2,1)S(1)}, u32[]{:S(2)}, u32[]{:S(2)}) collective-permute-start(bf16[4,88,384]{2,1,0:T(8,128)(2,1)S(1)} %get-tuple-element.36), channel_id=1, source_target_pairs={{0,128},{1,897},{2,130},{3,899},{4,132},{5,901},{6,134},{7,903},{8... | collective-permute-start | bytes 811016 | tf_op jit(solution)/shard_map/ppermute | solution.py:306
  68.9 2.3 %collective-permute-start.3 = (bf16[4,88,384]{2,1,0:T(8,128)(2,1)S(1)}, bf16[4,88,384]{2,1,0:T(8,128)(2,1)S(1)}, u32[]{:S(2)}, u32[]{:S(2)}) collective-permute-start(bf16[4,88,384]{2,1,0:T(8,128)(2,1)S(1)} %get-tuple-element.37), channel_id=1, source_target_pairs={{0,64},{1,961},{2,66},{3,963},{4,68},{5,965},{6,70},{7,967},{8,72}... | collective-permute-start | bytes 811016 | tf_op jit(solution)/shard_map/ppermute | solution.py:306
  71.2 11.7 %collective-permute-start.4 = (bf16[4,88,384]{2,1,0:T(8,128)(2,1)S(1)}, bf16[4,88,384]{2,1,0:T(8,128)(2,1)S(1)}, u32[]{:S(2)}, u32[]{:S(2)}) collective-permute-start(bf16[4,88,384]{2,1,0:T(8,128)(2,1)S(1)} %get-tuple-element.38), channel_id=1, source_target_pairs={{0,960},{1,65},{2,962},{3,67},{4,964},{5,69},{6,966},{7,71},{8,968... | collective-permute-start | bytes 811016 | tf_op jit(solution)/shard_map/ppermute | solution.py:306
  82.9 0.7 collective-permute-done.2.far_ref
  83.6 8.6 %collective-permute-done.3.near_ref = bf16[4,88,384]{2,1,0:T(8,128)(2,1)S(1)} collective-permute-done((bf16[4,88,384]{2,1,0:T(8,128)(2,1)S(1)}, bf16[4,88,384]{2,1,0:T(8,128)(2,1)S(1)}, u32[]{:S(2)}, u32[]{:S(2)}) %collective-permute-start.3) | collective-permute-done | bytes 270368 | tf_op jit(solution)/shard_map/ppermute | solution.py:306
  92.1 0.0 collective-permute-done.4.back_ref
  92.1 0.1 stop.1
  92.3 1.9 %collective-permute-start.5 = (bf16[88,384]{1,0:T(8,128)(2,1)S(1)}, bf16[88,384]{1,0:T(8,128)(2,1)S(1)}, u32[]{:S(2)}, u32[]{:S(2)}) collective-permute-start(bf16[88,384]{1,0:T(8,128)(2,1)S(1)} %get-tuple-element.41), channel_id=1, source_target_pairs={{0,256},{1,769},{2,258},{3,771},{4,260},{5,773},{6,262},{7,775},{8... | collective-permute-start | bytes 202760 | tf_op jit(solution)/shard_map/ppermute | solution.py:306
  94.2 11.4 %collective-permute-start.6 = (bf16[88,384]{1,0:T(8,128)(2,1)S(1)}, bf16[88,384]{1,0:T(8,128)(2,1)S(1)}, u32[]{:S(2)}, u32[]{:S(2)}) collective-permute-start(bf16[88,384]{1,0:T(8,128)(2,1)S(1)} %get-tuple-element.42), channel_id=1, source_target_pairs={{0,512},{1,513},{2,514},{3,515},{4,516},{5,517},{6,518},{7,519},{8... | collective-permute-start | bytes 202760 | tf_op jit(solution)/shard_map/ppermute | solution.py:306
  105.6 3.6 %collective-permute-start.7 = (bf16[88,384]{1,0:T(8,128)(2,1)S(1)}, bf16[88,384]{1,0:T(8,128)(2,1)S(1)}, u32[]{:S(2)}, u32[]{:S(2)}) collective-permute-start(bf16[88,384]{1,0:T(8,128)(2,1)S(1)} %get-tuple-element.43), channel_id=1, source_target_pairs={{0,768},{1,257},{2,770},{3,259},{4,772},{5,261},{6,774},{7,263},{8... | collective-permute-start | bytes 202760 | tf_op jit(solution)/shard_map/ppermute | solution.py:306
  109.2 0.0 collective-permute-done.5.b_ref
  109.3 1.9 %collective-permute-done.6.c_ref = bf16[88,384]{1,0:T(8,128)(2,1)S(1)} collective-permute-done((bf16[88,384]{1,0:T(8,128)(2,1)S(1)}, bf16[88,384]{1,0:T(8,128)(2,1)S(1)}, u32[]{:S(2)}, u32[]{:S(2)}) %collective-permute-start.6) | collective-permute-done | bytes 67616 | tf_op jit(solution)/shard_map/ppermute | solution.py:306
  111.2 6.3 %collective-permute-done.7.d_ref = bf16[88,384]{1,0:T(8,128)(2,1)S(1)} collective-permute-done((bf16[88,384]{1,0:T(8,128)(2,1)S(1)}, bf16[88,384]{1,0:T(8,128)(2,1)S(1)}, u32[]{:S(2)}, u32[]{:S(2)}) %collective-permute-start.7) | collective-permute-done | bytes 67616 | tf_op jit(solution)/shard_map/ppermute | solution.py:306
  117.5 0.0 all-to-all-done.2.part_ref
  117.5 0.0 copy-done.3
  117.5 0.0 copy-done.4
  117.5 0.3 owner.1
  117.9 32.8 %all-gather.1.all_ref = bf16[16,85,384]{2,1,0:T(8,128)(2,1)S(1)} all-gather(bf16[1,85,384]{2,1,0:T(8,128)(2,1)S(1)} %bitcast.15), channel_id=2, replica_groups=mesh['rep'=16,'fs'=8,'tp'=8] {'rep'}, dimensions={0}, use_global_device_ids=true | all-gather | bytes 1109760 | tf_op jit(solution)/shard_map/all_gather | solution.py:418
  150.6 1.5 out.1
  (1 shorter events, 0.0 us)
Async XLA Ops:
  21.3 24.5 %copy-start = (bf16[84,2048]{1,0:T(8,128)(2,1)S(1)}, bf16[84,2048]{1,0:T(8,128)(2,1)}, u32[]{:S(2)}) copy-start(bf16[84,2048]{1,0:T(8,128)(2,1)} %gate_w_ref.1) | copy-start | bytes 1032196
  21.3 24.5 %copy-start.1 = (bf16[84,2048]{1,0:T(8,128)(2,1)S(1)}, bf16[84,2048]{1,0:T(8,128)(2,1)}, u32[]{:S(2)}) copy-start(bf16[84,2048]{1,0:T(8,128)(2,1)} %up_w_ref.1) | copy-start | bytes 1032196
  21.3 24.5 %copy-start.2 = (bf16[84,2048]{1,0:T(8,128)(2,1)S(1)}, bf16[84,2048]{1,0:T(8,128)(2,1)}, u32[]{:S(2)}) copy-start(bf16[84,2048]{1,0:T(8,128)(2,1)} %down_w_ref.1) | copy-start | bytes 1032196
  21.3 24.5 %copy-start.5 = (f32[2048]{0:T(1024)S(1)}, f32[2048]{0:T(1024)}, u32[]{:S(2)}) copy-start(f32[2048]{0:T(1024)} %param.8) | copy-start | bytes 24580
  43.9 5.3 %collective-permute-start = (bf16[32,32,768]{2,1,0:T(8,128)(2,1)S(1)}, bf16[32,32,768]{2,1,0:T(8,128)(2,1)S(1)}, u32[]{:S(2)}, u32[]{:S(2)}) collective-permute-start(bf16[32,32,768]{2,1,0:T(8,128)(2,1)S(1)} %bitcast.8), channel_id=1, source_target_pairs={{0,1},{1,0},{2,3},{3,2},{4,5},{5,4},{6,7},{7,6},{8,9},{9,8},{10,11... | collective-permute-start | bytes 4718600 | tf_op jit(solution)/shard_map/ppermute | solution.py:296
  53.0 4.2 %collective-permute-start.1 = (bf16[33,32,384]{2,1,0:T(8,128)(2,1)S(1)}, bf16[33,32,384]{2,1,0:T(8,128)(2,1)S(1)}, u32[]{:S(2)}, u32[]{:S(2)}) collective-permute-start(bf16[33,32,384]{2,1,0:T(8,128)(2,1)S(1)} %get-tuple-element.33), channel_id=1, source_target_pairs={{0,1},{1,0},{2,3},{3,2},{4,5},{5,4},{6,7},{7,6},{8,9},{9,8},{10,11... | collective-permute-start | bytes 2433032 | tf_op jit(solution)/shard_map/ppermute | solution.py:296
  58.2 59.3 %copy-start.3 = (bf16[384,32]{0,1:T(8,128)(2,1)S(1)}, bf16[384,32]{0,1:T(8,128)(2,1)}, u32[]{:S(2)}) copy-start(bf16[384,32]{0,1:T(8,128)(2,1)} %param.7) | copy-start | bytes 73732
  58.2 59.3 %copy-start.4 = (bf16[384,32]{0,1:T(8,128)(2,1)S(1)}, bf16[384,32]{0,1:T(8,128)(2,1)}, u32[]{:S(2)}) copy-start(bf16[384,32]{0,1:T(8,128)(2,1)} %param.6) | copy-start | bytes 73732
  58.2 59.3 %all-to-all-start.2 = ((bf16[32,104,128]{2,1,0:T(8,128)(2,1)}), bf16[32,104,128]{2,1,0:T(8,128)(2,1)S(1)}, u32[]{:S(2)}, u32[]{:S(2)}) async-start(bf16[32,104,128]{2,1,0:T(8,128)(2,1)} %core.1), calls=%async_computation.2 | async-start | bytes 1703936 | tf_op jit(solution)/shard_map/all_to_all | solution.py:393
  67.0 16.6 %collective-permute-start.2 = (bf16[4,88,384]{2,1,0:T(8,128)(2,1)S(1)}, bf16[4,88,384]{2,1,0:T(8,128)(2,1)S(1)}, u32[]{:S(2)}, u32[]{:S(2)}) collective-permute-start(bf16[4,88,384]{2,1,0:T(8,128)(2,1)S(1)} %get-tuple-element.36), channel_id=1, source_target_pairs={{0,128},{1,897},{2,130},{3,899},{4,132},{5,901},{6,134},{7,903},{8... | collective-permute-start | bytes 811016 | tf_op jit(solution)/shard_map/ppermute | solution.py:306
  68.9 23.3 %collective-permute-start.3 = (bf16[4,88,384]{2,1,0:T(8,128)(2,1)S(1)}, bf16[4,88,384]{2,1,0:T(8,128)(2,1)S(1)}, u32[]{:S(2)}, u32[]{:S(2)}) collective-permute-start(bf16[4,88,384]{2,1,0:T(8,128)(2,1)S(1)} %get-tuple-element.37), channel_id=1, source_target_pairs={{0,64},{1,961},{2,66},{3,963},{4,68},{5,965},{6,70},{7,967},{8,72}... | collective-permute-start | bytes 811016 | tf_op jit(solution)/shard_map/ppermute | solution.py:306
  71.2 21.0 %collective-permute-start.4 = (bf16[4,88,384]{2,1,0:T(8,128)(2,1)S(1)}, bf16[4,88,384]{2,1,0:T(8,128)(2,1)S(1)}, u32[]{:S(2)}, u32[]{:S(2)}) collective-permute-start(bf16[4,88,384]{2,1,0:T(8,128)(2,1)S(1)} %get-tuple-element.38), channel_id=1, source_target_pairs={{0,960},{1,65},{2,962},{3,67},{4,964},{5,69},{6,966},{7,71},{8,968... | collective-permute-start | bytes 811016 | tf_op jit(solution)/shard_map/ppermute | solution.py:306
  92.3 17.0 %collective-permute-start.5 = (bf16[88,384]{1,0:T(8,128)(2,1)S(1)}, bf16[88,384]{1,0:T(8,128)(2,1)S(1)}, u32[]{:S(2)}, u32[]{:S(2)}) collective-permute-start(bf16[88,384]{1,0:T(8,128)(2,1)S(1)} %get-tuple-element.41), channel_id=1, source_target_pairs={{0,256},{1,769},{2,258},{3,771},{4,260},{5,773},{6,262},{7,775},{8... | collective-permute-start | bytes 202760 | tf_op jit(solution)/shard_map/ppermute | solution.py:306
  94.2 17.0 %collective-permute-start.6 = (bf16[88,384]{1,0:T(8,128)(2,1)S(1)}, bf16[88,384]{1,0:T(8,128)(2,1)S(1)}, u32[]{:S(2)}, u32[]{:S(2)}) collective-permute-start(bf16[88,384]{1,0:T(8,128)(2,1)S(1)} %get-tuple-element.42), channel_id=1, source_target_pairs={{0,512},{1,513},{2,514},{3,515},{4,516},{5,517},{6,518},{7,519},{8... | collective-permute-start | bytes 202760 | tf_op jit(solution)/shard_map/ppermute | solution.py:306
  105.6 11.9 %collective-permute-start.7 = (bf16[88,384]{1,0:T(8,128)(2,1)S(1)}, bf16[88,384]{1,0:T(8,128)(2,1)S(1)}, u32[]{:S(2)}, u32[]{:S(2)}) collective-permute-start(bf16[88,384]{1,0:T(8,128)(2,1)S(1)} %get-tuple-element.43), channel_id=1, source_target_pairs={{0,768},{1,257},{2,770},{3,259},{4,772},{5,261},{6,774},{7,263},{8... | collective-permute-start | bytes 202760 | tf_op jit(solution)/shard_map/ppermute | solution.py:306

commit v4 on v3

--- a/solution.py
+++ b/solution.py
@@ -141,7 +141,7 @@
 
     lax.fori_loop(0, n_fs * n_x, share, 0, unroll=4)
 
-    side = 1 - 2 * core
+    side = 2 * core - 1
     for b in range(width // step):
         rows = slice(b * step, (b + 1) * step)
         two = lax.dot_general(
@@ -301,7 +301,7 @@
     pairs = []
     for z in range(n):
         for k in range(m):
-            to = (z - by if k % 2 else z + by) % n
+            to = (z + by if k % 2 else z - by) % n
             pairs.append((z * m + k, to * m + k))
     return lax.ppermute(v, ("rep", "node"), pairs)
 
@@ -383,7 +383,7 @@
         out_specs=ANY,
         scratch_shapes=[
             pltpu.VMEM((peers, block * (rows // LANES) + 8, LANES), BF),
-            pltpu.SemaphoreType.DMA((4,)),
+            pltpu.SemaphoreType.DMA((8,)),
         ],
         compiler_params=pltpu.CompilerParams(vmem_limit_bytes=8 * 2**20),
         cost_estimate=pl.CostEstimate(flops=10**6, bytes_accessed=3 * 10**6, transcendentals=0),

time: 153 us -> 152 us (level)
  waiting for transfers between devices: 22.5 us -> 16.6 us
  blocking collectives: 75.1 us -> 79.8 us
    ppermute x6, waiting for transfers between devices: 17.5 us -> 11.6 us  [shifted(): return lax.ppermute(v, ('rep', 'node'), pairs)]
    all_gather x1, blocking collectives: 32.8 us -> 37.5 us  [body(): everything = lax.all_gather(chunk, 'rep', axis=0, tiled=False)]
  transfers between devices with their start and end apart: 9 -> 9, of which waited for: 6 -> 5; matrix products, arithmetic and copies ran while one was open for 0% -> 0% of each run, Pallas kernels for 0% -> 0%
where the time goes in v4:
time: 152 us
  blocking collectives  79.8 us (52%)
  starting transfers between devices  46.3 us (30%)
  waiting for transfers between devices  16.6 us (11%)
  Pallas kernels  7.27 us (5%)
    all_to_all x2, blocking collectives, spread(): lax.all_to_all(copies, 'node', 0, 0, tiled=True, axis_index_groups=groups)  42.3 us
    all_gather x1, blocking collectives, body(): everything = lax.all_gather(chunk, 'rep', axis=0, tiled=False)  37.5 us
    ppermute x6, starting transfers between devices, shifted(): return lax.ppermute(v, ('rep', 'node'), pairs)  33.6 us
    ppermute x6, waiting for transfers between devices, shifted(): return lax.ppermute(v, ('rep', 'node'), pairs)  11.6 us
    all_to_all x1, starting transfers between devices, body(): lax.all_to_all(ready, 'node', 0, 0, tiled=True, axis_index_groups=across)  8.7 us
    ppermute x2, waiting for transfers between devices, swapped(): return lax.ppermute(v, 'node', [(k, k ^ 1) for k in range(n)])  4.96 us
    ppermute x2, starting transfers between devices, swapped(): return lax.ppermute(v, 'node', [(k, k ^ 1) for k in range(n)])  3.95 us
    pallas_call x1, Pallas kernels, body(): pl.pallas_call(functools.partial(main_kernel, sizes), out_shape=[shape(pe...  3.8 us
  transfers between devices with their start and end apart: 9, of which 5 were waited for; matrix products, arithmetic and copies ran while one was open for 0% of the time, Pallas kernels for 0%

profile of v4, /device:TPU:6, one launch (start us, length us, event | category | flops | bytes accessed | tf_op | source)
XLA Modules:
  0.0 151.7 jit_solution(5044472379413738988)
XLA Ops:
  0.6 0.8 pad_maximum_fusion
  1.4 19.7 %all_to_all.15 = bf16[8,32,768]{2,1,0:T(8,128)(2,1)S(1)} all-to-all(bf16[8,32,768]{2,1,0:T(8,128)(2,1)S(1)} %broadcast_in_dim.6), channel_id=1, replica_groups={{36,32,20,16,4,0,52,48},{38,34,22,18,6,2,54,50},{44,40,28,24,12,8,60,56..., dimensions={0} | all-to-all | bytes 786432 | tf_op jit(solution)/shard_map/all_to_all | solution.py:271
  21.2 0.1 broadcast_in_dim.15
  21.3 0.0 copy-start
  21.3 0.0 copy-start.1
  21.3 0.0 copy-start.2
  21.3 0.0 copy-start.5
  21.3 22.6 %all_to_all.16 = bf16[4,256,768]{2,1,0:T(8,128)(2,1)S(1)} all-to-all(bf16[4,256,768]{2,1,0:T(8,128)(2,1)S(1)} %broadcast_in_dim.15), channel_id=1, replica_groups={{2,0,10,8},{6,4,14,12},{18,16,26,24},{22,20,30,28},{34,32,42,40},{38,36..., dimensions={0} | all-to-all | bytes 3145728 | tf_op jit(solution)/shard_map/all_to_all | solution.py:271
  43.9 1.9 %collective-permute-start = (bf16[32,32,768]{2,1,0:T(8,128)(2,1)S(1)}, bf16[32,32,768]{2,1,0:T(8,128)(2,1)S(1)}, u32[]{:S(2)}, u32[]{:S(2)}) collective-permute-start(bf16[32,32,768]{2,1,0:T(8,128)(2,1)S(1)} %bitcast.8), channel_id=1, source_target_pairs={{0,1},{1,0},{2,3},{3,2},{4,5},{5,4},{6,7},{7,6},{8,9},{9,8},{10,11... | collective-permute-start | bytes 4718600 | tf_op jit(solution)/shard_map/ppermute | solution.py:296
  45.8 0.0 copy-done
  45.8 0.0 copy-done.1
  45.8 0.0 copy-done.2
  45.8 0.0 copy-done.5
  45.9 0.5 ready.1
  46.4 2.8 %collective-permute-done.other_ref = bf16[32,32,768]{2,1,0:T(8,128)(2,1)S(1)} collective-permute-done((bf16[32,32,768]{2,1,0:T(8,128)(2,1)S(1)}, bf16[32,32,768]{2,1,0:T(8,128)(2,1)S(1)}, u32[]{:S(2)}, u32[]{:S(2)}) %collective-permute-start) | collective-permute-done | bytes 1572896 | tf_op jit(solution)/shard_map/ppermute | solution.py:296
  49.2 3.8 %main.1 = (bf16[32,32,384]{2,1,0:T(8,128)(2,1)S(1)}, bf16[33,32,384]{2,1,0:T(8,128)(2,1)S(1)}, f32[8,384]{1,0:T(8,128)S(1)}, f32[8,384]{1,0:T(8,128)S(1)}, bf16[...) custom-call(bf16[32,32,768]{2,1,0:T(8,128)(2,1)S(1)} %bitcast.10, ...), custom_call_target="tpu_custom_call" | custom-call | flops 1100000000 | bytes 10000000 | tf_op jit(solution)/shard_map/main/pallas_call | solution.py:348
  53.0 2.0 %collective-permute-start.1 = (bf16[33,32,384]{2,1,0:T(8,128)(2,1)S(1)}, bf16[33,32,384]{2,1,0:T(8,128)(2,1)S(1)}, u32[]{:S(2)}, u32[]{:S(2)}) collective-permute-start(bf16[33,32,384]{2,1,0:T(8,128)(2,1)S(1)} %get-tuple-element.33), channel_id=1, source_target_pairs={{0,1},{1,0},{2,3},{3,2},{4,5},{5,4},{6,7},{7,6},{8,9},{9,8},{10,11... | collective-permute-start | bytes 2433032 | tf_op jit(solution)/shard_map/ppermute | solution.py:296
  55.0 2.2 %collective-permute-done.1.got_ref = bf16[33,32,384]{2,1,0:T(8,128)(2,1)S(1)} collective-permute-done((bf16[33,32,384]{2,1,0:T(8,128)(2,1)S(1)}, bf16[33,32,384]{2,1,0:T(8,128)(2,1)S(1)}, u32[]{:S(2)}, u32[]{:S(2)}) %collective-permute-start.1) | collective-permute-done | bytes 811040 | tf_op jit(solution)/shard_map/ppermute | solution.py:296
  57.2 1.0 core.1
  58.2 0.0 copy-start.3
  58.2 0.0 copy-start.4
  58.3 8.7 %all-to-all-start.2 = ((bf16[32,104,128]{2,1,0:T(8,128)(2,1)}), bf16[32,104,128]{2,1,0:T(8,128)(2,1)S(1)}, u32[]{:S(2)}, u32[]{:S(2)}) async-start(bf16[32,104,128]{2,1,0:T(8,128)(2,1)} %core.1), calls=%async_computation.2 | async-start | bytes 1703936 | tf_op jit(solution)/shard_map/all_to_all | solution.py:393
  67.0 12.1 %collective-permute-start.2 = (bf16[4,88,384]{2,1,0:T(8,128)(2,1)S(1)}, bf16[4,88,384]{2,1,0:T(8,128)(2,1)S(1)}, u32[]{:S(2)}, u32[]{:S(2)}) collective-permute-start(bf16[4,88,384]{2,1,0:T(8,128)(2,1)S(1)} %get-tuple-element.36), channel_id=1, source_target_pairs={{0,896},{1,129},{2,898},{3,131},{4,900},{5,133},{6,902},{7,135},{8... | collective-permute-start | bytes 811016 | tf_op jit(solution)/shard_map/ppermute | solution.py:306
  79.0 2.5 %collective-permute-start.3 = (bf16[4,88,384]{2,1,0:T(8,128)(2,1)S(1)}, bf16[4,88,384]{2,1,0:T(8,128)(2,1)S(1)}, u32[]{:S(2)}, u32[]{:S(2)}) collective-permute-start(bf16[4,88,384]{2,1,0:T(8,128)(2,1)S(1)} %get-tuple-element.37), channel_id=1, source_target_pairs={{0,960},{1,65},{2,962},{3,67},{4,964},{5,69},{6,966},{7,71},{8,968... | collective-permute-start | bytes 811016 | tf_op jit(solution)/shard_map/ppermute | solution.py:306
  81.5 3.4 %collective-permute-start.4 = (bf16[4,88,384]{2,1,0:T(8,128)(2,1)S(1)}, bf16[4,88,384]{2,1,0:T(8,128)(2,1)S(1)}, u32[]{:S(2)}, u32[]{:S(2)}) collective-permute-start(bf16[4,88,384]{2,1,0:T(8,128)(2,1)S(1)} %get-tuple-element.38), channel_id=1, source_target_pairs={{0,64},{1,961},{2,66},{3,963},{4,68},{5,965},{6,70},{7,967},{8,72}... | collective-permute-start | bytes 811016 | tf_op jit(solution)/shard_map/ppermute | solution.py:306
  84.9 2.9 %collective-permute-done.2.far_ref = bf16[4,88,384]{2,1,0:T(8,128)(2,1)S(1)} collective-permute-done((bf16[4,88,384]{2,1,0:T(8,128)(2,1)S(1)}, bf16[4,88,384]{2,1,0:T(8,128)(2,1)S(1)}, u32[]{:S(2)}, u32[]{:S(2)}) %collective-permute-start.2) | collective-permute-done | bytes 270368 | tf_op jit(solution)/shard_map/ppermute | solution.py:306
  87.8 3.9 %collective-permute-done.3.near_ref = bf16[4,88,384]{2,1,0:T(8,128)(2,1)S(1)} collective-permute-done((bf16[4,88,384]{2,1,0:T(8,128)(2,1)S(1)}, bf16[4,88,384]{2,1,0:T(8,128)(2,1)S(1)}, u32[]{:S(2)}, u32[]{:S(2)}) %collective-permute-start.3) | collective-permute-done | bytes 270368 | tf_op jit(solution)/shard_map/ppermute | solution.py:306
  91.7 0.0 collective-permute-done.4.back_ref
  91.7 0.1 stop.1
  91.8 5.3 %collective-permute-start.5 = (bf16[88,384]{1,0:T(8,128)(2,1)S(1)}, bf16[88,384]{1,0:T(8,128)(2,1)S(1)}, u32[]{:S(2)}, u32[]{:S(2)}) collective-permute-start(bf16[88,384]{1,0:T(8,128)(2,1)S(1)} %get-tuple-element.41), channel_id=1, source_target_pairs={{0,768},{1,257},{2,770},{3,259},{4,772},{5,261},{6,774},{7,263},{8... | collective-permute-start | bytes 202760 | tf_op jit(solution)/shard_map/ppermute | solution.py:306
  97.1 2.6 %collective-permute-start.6 = (bf16[88,384]{1,0:T(8,128)(2,1)S(1)}, bf16[88,384]{1,0:T(8,128)(2,1)S(1)}, u32[]{:S(2)}, u32[]{:S(2)}) collective-permute-start(bf16[88,384]{1,0:T(8,128)(2,1)S(1)} %get-tuple-element.42), channel_id=1, source_target_pairs={{0,512},{1,513},{2,514},{3,515},{4,516},{5,517},{6,518},{7,519},{8... | collective-permute-start | bytes 202760 | tf_op jit(solution)/shard_map/ppermute | solution.py:306
  99.7 7.8 %collective-permute-start.7 = (bf16[88,384]{1,0:T(8,128)(2,1)S(1)}, bf16[88,384]{1,0:T(8,128)(2,1)S(1)}, u32[]{:S(2)}, u32[]{:S(2)}) collective-permute-start(bf16[88,384]{1,0:T(8,128)(2,1)S(1)} %get-tuple-element.43), channel_id=1, source_target_pairs={{0,256},{1,769},{2,258},{3,771},{4,260},{5,773},{6,262},{7,775},{8... | collective-permute-start | bytes 202760 | tf_op jit(solution)/shard_map/ppermute | solution.py:306
  107.6 0.0 collective-permute-done.5.b_ref
  107.6 4.8 %collective-permute-done.6.c_ref = bf16[88,384]{1,0:T(8,128)(2,1)S(1)} collective-permute-done((bf16[88,384]{1,0:T(8,128)(2,1)S(1)}, bf16[88,384]{1,0:T(8,128)(2,1)S(1)}, u32[]{:S(2)}, u32[]{:S(2)}) %collective-permute-start.6) | collective-permute-done | bytes 67616 | tf_op jit(solution)/shard_map/ppermute | solution.py:306
  112.4 0.0 collective-permute-done.7.d_ref
  112.4 0.0 all-to-all-done.2.part_ref
  112.4 0.0 copy-done.3
  112.4 0.0 copy-done.4
  112.4 0.3 owner.1
  112.8 37.5 %all-gather.1.all_ref = bf16[16,85,384]{2,1,0:T(8,128)(2,1)S(1)} all-gather(bf16[1,85,384]{2,1,0:T(8,128)(2,1)S(1)} %bitcast.15), channel_id=2, replica_groups=mesh['rep'=16,'fs'=8,'tp'=8] {'rep'}, dimensions={0}, use_global_device_ids=true | all-gather | bytes 1109760 | tf_op jit(solution)/shard_map/all_gather | solution.py:418
  150.2 1.5 out.1
  (1 shorter events, 0.0 us)
Async XLA Ops:
  21.3 24.5 %copy-start = (bf16[84,2048]{1,0:T(8,128)(2,1)S(1)}, bf16[84,2048]{1,0:T(8,128)(2,1)}, u32[]{:S(2)}) copy-start(bf16[84,2048]{1,0:T(8,128)(2,1)} %gate_w_ref.1) | copy-start | bytes 1032196
  21.3 24.5 %copy-start.1 = (bf16[84,2048]{1,0:T(8,128)(2,1)S(1)}, bf16[84,2048]{1,0:T(8,128)(2,1)}, u32[]{:S(2)}) copy-start(bf16[84,2048]{1,0:T(8,128)(2,1)} %up_w_ref.1) | copy-start | bytes 1032196
  21.3 24.5 %copy-start.2 = (bf16[84,2048]{1,0:T(8,128)(2,1)S(1)}, bf16[84,2048]{1,0:T(8,128)(2,1)}, u32[]{:S(2)}) copy-start(bf16[84,2048]{1,0:T(8,128)(2,1)} %down_w_ref.1) | copy-start | bytes 1032196
  21.3 24.5 %copy-start.5 = (f32[2048]{0:T(1024)S(1)}, f32[2048]{0:T(1024)}, u32[]{:S(2)}) copy-start(f32[2048]{0:T(1024)} %param.8) | copy-start | bytes 24580
  43.9 5.3 %collective-permute-start = (bf16[32,32,768]{2,1,0:T(8,128)(2,1)S(1)}, bf16[32,32,768]{2,1,0:T(8,128)(2,1)S(1)}, u32[]{:S(2)}, u32[]{:S(2)}) collective-permute-start(bf16[32,32,768]{2,1,0:T(8,128)(2,1)S(1)} %bitcast.8), channel_id=1, source_target_pairs={{0,1},{1,0},{2,3},{3,2},{4,5},{5,4},{6,7},{7,6},{8,9},{9,8},{10,11... | collective-permute-start | bytes 4718600 | tf_op jit(solution)/shard_map/ppermute | solution.py:296
  53.0 4.2 %collective-permute-start.1 = (bf16[33,32,384]{2,1,0:T(8,128)(2,1)S(1)}, bf16[33,32,384]{2,1,0:T(8,128)(2,1)S(1)}, u32[]{:S(2)}, u32[]{:S(2)}) collective-permute-start(bf16[33,32,384]{2,1,0:T(8,128)(2,1)S(1)} %get-tuple-element.33), channel_id=1, source_target_pairs={{0,1},{1,0},{2,3},{3,2},{4,5},{5,4},{6,7},{7,6},{8,9},{9,8},{10,11... | collective-permute-start | bytes 2433032 | tf_op jit(solution)/shard_map/ppermute | solution.py:296
  58.2 54.2 %copy-start.3 = (bf16[384,32]{0,1:T(8,128)(2,1)S(1)}, bf16[384,32]{0,1:T(8,128)(2,1)}, u32[]{:S(2)}) copy-start(bf16[384,32]{0,1:T(8,128)(2,1)} %param.7) | copy-start | bytes 73732
  58.2 54.2 %copy-start.4 = (bf16[384,32]{0,1:T(8,128)(2,1)S(1)}, bf16[384,32]{0,1:T(8,128)(2,1)}, u32[]{:S(2)}) copy-start(bf16[384,32]{0,1:T(8,128)(2,1)} %param.6) | copy-start | bytes 73732
  58.3 54.2 %all-to-all-start.2 = ((bf16[32,104,128]{2,1,0:T(8,128)(2,1)}), bf16[32,104,128]{2,1,0:T(8,128)(2,1)S(1)}, u32[]{:S(2)}, u32[]{:S(2)}) async-start(bf16[32,104,128]{2,1,0:T(8,128)(2,1)} %core.1), calls=%async_computation.2 | async-start | bytes 1703936 | tf_op jit(solution)/shard_map/all_to_all | solution.py:393
  67.0 20.8 %collective-permute-start.2 = (bf16[4,88,384]{2,1,0:T(8,128)(2,1)S(1)}, bf16[4,88,384]{2,1,0:T(8,128)(2,1)S(1)}, u32[]{:S(2)}, u32[]{:S(2)}) collective-permute-start(bf16[4,88,384]{2,1,0:T(8,128)(2,1)S(1)} %get-tuple-element.36), channel_id=1, source_target_pairs={{0,896},{1,129},{2,898},{3,131},{4,900},{5,133},{6,902},{7,135},{8... | collective-permute-start | bytes 811016 | tf_op jit(solution)/shard_map/ppermute | solution.py:306
  79.0 12.6 %collective-permute-start.3 = (bf16[4,88,384]{2,1,0:T(8,128)(2,1)S(1)}, bf16[4,88,384]{2,1,0:T(8,128)(2,1)S(1)}, u32[]{:S(2)}, u32[]{:S(2)}) collective-permute-start(bf16[4,88,384]{2,1,0:T(8,128)(2,1)S(1)} %get-tuple-element.37), channel_id=1, source_target_pairs={{0,960},{1,65},{2,962},{3,67},{4,964},{5,69},{6,966},{7,71},{8,968... | collective-permute-start | bytes 811016 | tf_op jit(solution)/shard_map/ppermute | solution.py:306
  81.5 10.2 %collective-permute-start.4 = (bf16[4,88,384]{2,1,0:T(8,128)(2,1)S(1)}, bf16[4,88,384]{2,1,0:T(8,128)(2,1)S(1)}, u32[]{:S(2)}, u32[]{:S(2)}) collective-permute-start(bf16[4,88,384]{2,1,0:T(8,128)(2,1)S(1)} %get-tuple-element.38), channel_id=1, source_target_pairs={{0,64},{1,961},{2,66},{3,963},{4,68},{5,965},{6,70},{7,967},{8,72}... | collective-permute-start | bytes 811016 | tf_op jit(solution)/shard_map/ppermute | solution.py:306
  91.8 15.8 %collective-permute-start.5 = (bf16[88,384]{1,0:T(8,128)(2,1)S(1)}, bf16[88,384]{1,0:T(8,128)(2,1)S(1)}, u32[]{:S(2)}, u32[]{:S(2)}) collective-permute-start(bf16[88,384]{1,0:T(8,128)(2,1)S(1)} %get-tuple-element.41), channel_id=1, source_target_pairs={{0,768},{1,257},{2,770},{3,259},{4,772},{5,261},{6,774},{7,263},{8... | collective-permute-start | bytes 202760 | tf_op jit(solution)/shard_map/ppermute | solution.py:306
  97.1 15.3 %collective-permute-start.6 = (bf16[88,384]{1,0:T(8,128)(2,1)S(1)}, bf16[88,384]{1,0:T(8,128)(2,1)S(1)}, u32[]{:S(2)}, u32[]{:S(2)}) collective-permute-start(bf16[88,384]{1,0:T(8,128)(2,1)S(1)} %get-tuple-element.42), channel_id=1, source_target_pairs={{0,512},{1,513},{2,514},{3,515},{4,516},{5,517},{6,518},{7,519},{8... | collective-permute-start | bytes 202760 | tf_op jit(solution)/shard_map/ppermute | solution.py:306
  99.7 12.7 %collective-permute-start.7 = (bf16[88,384]{1,0:T(8,128)(2,1)S(1)}, bf16[88,384]{1,0:T(8,128)(2,1)S(1)}, u32[]{:S(2)}, u32[]{:S(2)}) collective-permute-start(bf16[88,384]{1,0:T(8,128)(2,1)S(1)} %get-tuple-element.43), channel_id=1, source_target_pairs={{0,256},{1,769},{2,258},{3,771},{4,260},{5,773},{6,262},{7,775},{8... | collective-permute-start | bytes 202760 | tf_op jit(solution)/shard_map/ppermute | solution.py:306
